TPU v7x, 512 devices: a whole 4x8x8 slice. The times are simulated.
512 devices in a mesh: ep: 32 (over z, x), tp: 16 (over y, core).
Axes of the slice: x: 4, y: 8, z: 8, core: 2. Of those that a mesh axis runs over, the one named last changes fastest.
Arguments:
- tokens_a: bfloat16 [4096, 2048], P('ep'), may hold values from -6 to 6
- gain_a: float32 [2048], replicated, may hold values from 0.1 to 1.9
- value_w: bfloat16 [2048, 2048], P(None, 'tp'), may hold values from -0.125 to 0.125
- gate_w: bfloat16 [2048, 2048], P(None, 'tp'), may hold values from -0.125 to 0.125
- kernel: float32 [31, 2048], P(None, 'tp')
- chan_gain: float32 [2048], P('tp'), may hold values from 0.1 to 1.9
- out_w: bfloat16 [2048, 2048], P('tp'), may hold values from -0.125 to 0.125
- tokens_b: bfloat16 [6144, 2048], P('ep'), may hold values from -6 to 6
- gain_b: float32 [2048], replicated, may hold values from 0.1 to 1.9
- routes: int32 [6144, 2], P('ep'), may hold values from 0 to 31, all different within a row; in each aligned block of 192 rows (0 to 191, 192 to 383, ...) at most 18 rows name the same one
- route_logits: float32 [6144, 2], P('ep'), may hold values from -6 to 6
- expert_gate: bfloat16 [32, 2048, 2816], P('ep', None, 'tp'), may hold values from -0.125 to 0.125
- expert_up: bfloat16 [32, 2048, 2816], P('ep', None, 'tp'), may hold values from -0.125 to 0.125
- expert_down: bfloat16 [32, 2816, 2048], P('ep', 'tp'), may hold values from -0.109375 to 0.109375
Outputs:
- conv_out: bfloat16 [2048, 4096], P('tp', 'ep')
- moe_out: bfloat16 [2048, 6144], P('tp', 'ep')
Inputs may be any that keep to these rules, and one draw needn't show every extreme that they name: `routes`: each row names 2 different experts; among the rows of one index of ep no expert is named by more than 18 rows, a bound that some block reaches.
All inputs are finite; a program needn't handle non-finite values.
Results may differ from a plain program's by a relative error of at most 0.018.
Values may be sent and summed in bfloat16 or wider, within the bound.
A program may use at most 64 MiB of HBM per device.

v0:
```python
import jax
import jax.numpy as jnp
from jax import lax
from jax.sharding import Mesh
from jax.sharding import PartitionSpec as P

CONV_CH = 2048
TP = ("tp_0", "tp_1")


def from_behind(block, axis, distance):
    devices = range(lax.axis_size(axis))
    route = [(i - distance, i) for i in devices if i - distance in devices]
    return lax.ppermute(block, axis, route)


def copy_for_each(x, axis):
    peers = lax.axis_size(axis)
    return lax.all_to_all(jnp.broadcast_to(x[None], (peers, *x.shape)), axis, 0, 0, tiled=True)


def taken_together(x, axis):
    return copy_for_each(x, axis).sum(axis=0)


def in_one(arrays, axis):
    ends = [0]
    for a in arrays:
        ends.append(ends[-1] + a.size)
    so_far = taken_together(jnp.concatenate([a.ravel() for a in arrays]), axis)
    return tuple((so_far[b:e].reshape(a.shape) for a, b, e in zip(arrays, ends, ends[1:])))


def in_blocks(x, dim, peers):
    before, after = (x.shape[:dim], x.shape[dim + 1 :])
    return jnp.moveaxis(x.reshape(*before, peers, -1, *after), dim, 0)


def sum_at_owner(x, axis, dim):
    peers = lax.axis_size(axis)
    tiles = lax.all_to_all(in_blocks(x, dim, peers), axis, 0, 0, tiled=True)
    return jnp.sum(tiles.astype(jnp.float32), axis=0)


def summed_rows(terms, axes):
    so_far = terms.astype(jnp.bfloat16)
    for axis in axes:
        so_far = lax.psum_scatter(so_far, axis, scatter_dimension=0, tiled=True)
    return so_far.astype(jnp.float32)


def rms_scaled(tokens, gain):
    values = tokens.astype(jnp.float32)
    scaled = values * lax.rsqrt(jnp.mean(values * values, axis=1, keepdims=True) + 1e-06)
    return (scaled * gain[None, :]).astype(jnp.bfloat16)


def slot_table(route_rows, experts, capacity):
    flat_expert = route_rows.reshape(-1)
    expert_ids = jnp.arange(experts, dtype=jnp.int32)
    onehot = (flat_expert[:, None] == expert_ids[None, :]).astype(jnp.int32)
    before = jnp.cumsum(onehot, axis=0) - onehot
    ranking = jnp.sum(before * onehot, axis=1)
    return flat_expert * capacity + ranking


def body(
    tokens_a,
    gain_a,
    value_w,
    gate_w,
    kernel,
    chan_gain,
    out_w,
    tokens_b,
    gain_b,
    routes,
    route_logits,
    expert_gate,
    expert_up,
    expert_down,
):
    normed = rms_scaled(tokens_a, gain_a)
    contract_first = (((0,), (1,)), ((), ()))
    value_part = lax.dot_general(
        value_w, normed, contract_first, preferred_element_type=jnp.float32
    )
    gate_part = lax.dot_general(gate_w, normed, contract_first, preferred_element_type=jnp.float32)
    glu = (value_part * jax.nn.sigmoid(gate_part)).astype(jnp.bfloat16)
    taps = kernel.shape[0]
    length = glu.shape[1]
    rim = from_behind(glu[:, length - (taps - 1) :], "ep", 1)
    padded = jnp.concatenate([rim, glu], axis=1).astype(jnp.float32)
    mixed = jnp.zeros(glu.shape, jnp.float32)
    for tap in range(taps):
        mixed = mixed + kernel[tap][:, None] * padded[:, tap : tap + length]
    chan_total, chan_square = in_one((jnp.sum(mixed, axis=0), jnp.sum(mixed * mixed, axis=0)), TP)
    average = chan_total / CONV_CH
    spread = chan_square / CONV_CH - average * average
    normal_out = (
        (mixed - average[None, :]) * lax.rsqrt(spread + 1e-05)[None, :] * chan_gain[:, None]
    )
    activated = jax.nn.silu(normal_out).astype(jnp.bfloat16)
    block_w = out_w
    conv_out = sum_at_owner(
        lax.dot_general(
            block_w, activated, (((0,), (0,)), ((), ())), preferred_element_type=jnp.float32
        ).astype(jnp.bfloat16),
        TP,
        0,
    ).astype(jnp.bfloat16)
    normed_b = rms_scaled(tokens_b, gain_b)
    experts = lax.axis_size("ep")
    token_count = tokens_b.shape[0]
    choices_per = routes.shape[1]
    capacity = 3 * token_count * choices_per // (2 * experts)
    slots = slot_table(routes, experts, capacity)
    owner = jnp.arange(slots.shape[0], dtype=jnp.int32) // choices_per
    filled = jnp.zeros((experts * capacity,), jnp.int32).at[slots].set(owner + 1)
    picked = jnp.take(normed_b, jnp.maximum(filled - 1, 0), axis=0)
    send_rows = jnp.where((filled > 0)[:, None], picked, jnp.zeros_like(picked)).reshape(
        experts, capacity, -1
    )
    weights = jax.nn.softmax(route_logits, axis=1).reshape(-1)
    slot_ids = jnp.arange(experts * capacity, dtype=jnp.int32)
    combine = (
        ((slots[:, None] == slot_ids[None, :]).astype(jnp.float32) * weights[:, None])
        .reshape(token_count, choices_per, -1)
        .sum(axis=1)
    )
    gate_local = expert_gate[0]
    up_local = expert_up[0]
    arrived = lax.all_to_all(send_rows, "ep", split_axis=0, concat_axis=0, tiled=True).reshape(
        experts * capacity, -1
    )
    gate_act = jnp.dot(arrived, gate_local, preferred_element_type=jnp.float32)
    up_act = jnp.dot(arrived, up_local, preferred_element_type=jnp.float32)
    hidden = (jax.nn.silu(gate_act) * up_act).astype(jnp.bfloat16)
    down_local = expert_down[0]
    block_w = down_local
    expert_rows = summed_rows(
        lax.dot_general(
            block_w, hidden, (((0,), (1,)), ((), ())), preferred_element_type=jnp.float32
        ),
        TP,
    ).astype(jnp.bfloat16)
    returned = lax.all_to_all(
        expert_rows.reshape(expert_rows.shape[0], experts, capacity),
        "ep",
        split_axis=1,
        concat_axis=1,
        tiled=True,
    )
    returned_flat = returned.reshape(returned.shape[0], -1).astype(jnp.float32)
    moe_out = lax.dot_general(
        returned_flat,
        combine,
        (((1,), (1,)), ((), ())),
        precision=lax.Precision.HIGHEST,
        preferred_element_type=jnp.float32,
    )
    return (conv_out, moe_out.astype(jnp.bfloat16))


def solution(mesh):
    finer = Mesh(mesh.devices.reshape(mesh.shape["ep"], 8, 2), ("ep", "tp_0", "tp_1"))
    return jax.shard_map(
        body,
        mesh=finer,
        in_specs=(
            P("ep", None),
            P(),
            P(None, TP),
            P(None, TP),
            P(None, TP),
            P(TP),
            P(TP, None),
            P("ep", None),
            P(),
            P("ep", None),
            P("ep", None),
            P("ep", None, TP),
            P("ep", None, TP),
            P("ep", TP, None),
        ),
        out_specs=(P(TP, "ep"), P(TP, "ep")),
        check_vma=False,
    )
```

profile of v0, /device:TPU:1, one launch (start us, length us, event | category | flops | bytes accessed | tf_op | source)
XLA Modules:
  0.0 225.8 jit_solution(308483901481874880)
XLA Ops:
  7.2 0.9 copy.52
  8.5 0.9 reduce-window.6
  10.0 2.9 %scatter_custom_fusion = s32[576]{0:T(1024)S(1)} fusion(s32[384]{0:T(512)S(1)} %fusion.71, s32[384]{0:T(512)S(1)} %fusion.65, s32[]{:T(128)} %constant.66.clone.1), kind=kCustom, calls=%fused_computation.131 | custom fusion | bytes 2308 | tf_op jit(solution)/shard_map/scatter | solution.py:119
  13.2 1.4 fusion.1
  14.6 0.9 fusion.3
  15.6 4.0 %gather_fusion = bf16[576,2048]{1,0:T(8,128)(2,1)} fusion(bf16[192,2048]{1,0:T(8,128)(2,1)S(1)} %fusion.3, s32[1024]{0:T(1024)S(1)} %pad_clamp_fusion), kind=kCustom, calls=%fused_computation | custom fusion | bytes 4720896 | tf_op jit(solution)/shard_map/jit(_take)/gather | solution.py:120
  19.6 4.3 %gather.7 = bf16[32,18,2048]{2,1,0:T(8,128)(2,1)} reshape(bf16[576,2048]{1,0:T(8,128)(2,1)} %gather_fusion) | data formatting | bytes 4718592 | tf_op jit(solution)/shard_map/jit(_take)/gather | solution.py:120
  23.8 2.2 select_select_fusion
  26.0 84.7 %all_to_all.21 = bf16[32,18,2048]{2,1,0:T(8,128)(2,1)} all-to-all(bf16[32,18,2048]{2,1,0:T(8,128)(2,1)S(1)} %select_select_fusion), channel_id=1, replica_groups=mesh['ep'=32,'tp_0'=8,'tp_1'=2] {'ep'}, dimensions={0} | all-to-all | bytes 4718592 | tf_op jit(solution)/shard_map/all_to_all | solution.py:133
  110.8 2.9 %reshape.162 = bf16[576,2048]{1,0:T(8,128)(2,1)S(1)} reshape(bf16[32,18,2048]{2,1,0:T(8,128)(2,1)} %all_to_all.21) | data formatting | bytes 4718592 | tf_op jit(solution)/shard_map/reshape | solution.py:133
  113.7 2.9 %fusion.17 = f32[576,176]{0,1:T(8,128)} fusion(bf16[576,2048]{1,0:T(8,128)(2,1)S(1)} %reshape.162, bf16[1,2048,176]{1,2,0:T(8,128)(2,1)} %param.25), kind=kOutput, calls=%fused_computation.31 | convolution fusion | flops 415236096 | bytes 3485696 | tf_op jit(solution)/shard_map/dot_general | solution.py:136
  116.6 4.7 %fusion = bf16[2048,576]{0,1:T(8,128)(2,1)} fusion(bf16[576,2048]{1,0:T(8,128)(2,1)S(1)} %reshape.162, bf16[1,176,2048]{2,1,0:T(8,128)(2,1)S(1)} %copy-done, bf16[1,2048,176]{1,2,0:T(8,128)(2,1)} %param.26, f32[576,176]{0,1:T(8,128)} %fusion.17), kind=kOutput, calls=%fused_computation.4 | convolution fusion | flops 832260096 | bytes 6565888 | tf_op jit(solution)/shard_map/dot_general | solution.py:142
  121.4 1.0 copy-done.3
  123.5 3.7 %collective-permute-start = (bf16[128,30]{0,1:T(8,128)(2,1)S(1)}, bf16[128,30]{0,1:T(8,128)(2,1)S(1)}, u32[]{:S(2)}, u32[]{:S(2)}) collective-permute-start(bf16[128,30]{0,1:T(8,128)(2,1)S(1)} %slice.270), channel_id=1, source_target_pairs={{0,16},{16,32},{32,48},{48,64},{64,80},{80,96},{96,112},{112,128},... | collective-permute-start | bytes 23048 | tf_op jit(solution)/shard_map/ppermute | solution.py:14
  128.4 17.9 %all_to_all.22 = f32[16,1,256]{2,1,0:T(1,128)S(1)} all-to-all(f32[16,1,256]{2,1,0:T(1,128)S(1)} %broadcast_in_dim.28), channel_id=1, replica_groups=mesh['ep'=32,'tp_0'=8,'tp_1'=2] {'tp_0','tp_1'}, dimensions={0} | all-to-all | bytes 32768 | tf_op jit(solution)/shard_map/all_to_all | solution.py:19
  146.7 0.9 copy.69
  147.6 3.7 %all-to-all-start.1 = ((bf16[16,128,128]{1,2,0:T(8,128)(2,1)}), bf16[16,128,128]{1,2,0:T(8,128)(2,1)S(1)}, u32[]{:S(2)}, u32[]{:S(2)}) async-start(bf16[16,128,128]{1,2,0:T(8,128)(2,1)} %bitcast.112), calls=%async_computation.1 | async-start | bytes 1048576 | tf_op jit(solution)/shard_map/all_to_all | solution.py:41
  151.4 21.0 %reduce-scatter.5.cloned.1.call-done = bf16[256,576]{0,1:T(8,128)(2,1)} async-done(((bf16[2048,576]{0,1:T(8,128)(2,1)}), bf16[256,576]{0,1:T(8,128)(2,1)}) %reduce-scatter.5.cloned.1.call-update) | async-done | bytes 294928 | tf_op jit(solution)/shard_map/reduce_scatter | solution.py:48
  172.4 1.8 copy.59
  174.4 22.2 %reduce-scatter.7.cloned.1.call-done = bf16[128,576]{1,0:T(8,128)(2,1)} async-done(((bf16[256,576]{1,0:T(8,128)(2,1)}), bf16[128,576]{1,0:T(8,128)(2,1)}) %reduce-scatter.7.cloned.1.call-update) | async-done | bytes 147472
  196.6 1.1 copy.60
  198.4 8.9 %all-to-all-start.3 = ((bf16[128,32,18]{0,2,1:T(8,128)(2,1)}), bf16[128,32,18]{0,2,1:T(8,128)(2,1)S(1)}, u32[]{:S(2)}, u32[]{:S(2)}) async-start(bf16[128,32,18]{0,2,1:T(8,128)(2,1)} %reshape.163), calls=%async_computation.4 | async-start | bytes 393216 | tf_op jit(solution)/shard_map/all_to_all | solution.py:147
  208.3 9.6 %all-to-all-done.3 = bf16[128,32,18]{0,2,1:T(8,128)(2,1)S(1)} async-done(((bf16[128,32,18]{0,2,1:T(8,128)(2,1)}), bf16[128,32,18]{0,2,1:T(8,128)(2,1)S(1)}, u32[]{:S(2)}, u32[]{:S(2)}) %all-to-all-start.3) | async-done | bytes 147488 | tf_op jit(solution)/shard_map/all_to_all | solution.py:147
  218.0 1.0 convolution_convert_fusion.2
  (66 shorter events, 5.8 us)
Async XLA Ops:
  7.2 109.4 %copy-start = (bf16[1,176,2048]{2,1,0:T(8,128)(2,1)S(1)}, bf16[1,176,2048]{2,1,0:T(8,128)(2,1)}, u32[]{:S(2)}) copy-start(bf16[1,176,2048]{2,1,0:T(8,128)(2,1)} %param.27) | copy-start | bytes 2162692
  7.2 7.4 %copy-start.1 = (bf16[192,2048]{1,0:T(8,128)(2,1)S(1)}, bf16[192,2048]{1,0:T(8,128)(2,1)}, u32[]{:S(2)}) copy-start(bf16[192,2048]{1,0:T(8,128)(2,1)} %param.21) | copy-start | bytes 2359300
  7.2 165.2 %reduce-scatter.5.cloned.1.call-start = ((), (), s32[]{:S(2)}) async-start(), calls=%async_computation.6 | async-start | bytes 2654208 | tf_op jit(solution)/shard_map/reduce_scatter | solution.py:48
  121.3 1.0 copy-start.3
  121.3 1.2 copy-start.7
  121.3 1.2 copy-start.9
  121.3 1.8 copy-start.8
  122.4 4.9 %copy-start.5 = (f32[31,128]{1,0:T(8,128)S(1)}, f32[31,128]{1,0:T(8,128)}, u32[]{:S(2)}) copy-start(f32[31,128]{1,0:T(8,128)} %param.18) | copy-start | bytes 47620
  122.6 23.7 %copy-start.2 = (bf16[128,2048]{1,0:T(8,128)(2,1)S(1)}, bf16[128,2048]{1,0:T(8,128)(2,1)}, u32[]{:S(2)}) copy-start(bf16[128,2048]{1,0:T(8,128)(2,1)} %param.20) | copy-start | bytes 1572868
  122.6 23.7 %copy-start.6 = (f32[128]{0:T(128)S(1)}, f32[128]{0:T(128)}, u32[]{:S(2)}) copy-start(f32[128]{0:T(128)} %param.19) | copy-start | bytes 1540
  123.5 4.5 %collective-permute-start = (bf16[128,30]{0,1:T(8,128)(2,1)S(1)}, bf16[128,30]{0,1:T(8,128)(2,1)S(1)}, u32[]{:S(2)}, u32[]{:S(2)}) collective-permute-start(bf16[128,30]{0,1:T(8,128)(2,1)S(1)} %slice.270), channel_id=1, source_target_pairs={{0,16},{16,32},{32,48},{48,64},{64,80},{80,96},{96,112},{112,128},... | collective-permute-start | bytes 23048 | tf_op jit(solution)/shard_map/ppermute | solution.py:14
  128.3 46.0 %copy-start.4 = (f32[192,2]{0,1:T(2,128)S(1)}, f32[192,2]{0,1:T(2,128)}, u32[]{:S(2)}) copy-start(f32[192,2]{0,1:T(2,128)} %param.24) | copy-start | bytes 4612
  147.6 50.8 %all-to-all-start.1 = ((bf16[16,128,128]{1,2,0:T(8,128)(2,1)}), bf16[16,128,128]{1,2,0:T(8,128)(2,1)S(1)}, u32[]{:S(2)}, u32[]{:S(2)}) async-start(bf16[16,128,128]{1,2,0:T(8,128)(2,1)} %bitcast.112), calls=%async_computation.1 | async-start | bytes 1048576 | tf_op jit(solution)/shard_map/all_to_all | solution.py:41
  151.4 45.2 %reduce-scatter.7.cloned.1.call-start = ((), (), s32[]{:S(2)}) async-start(), calls=%async_computation.7 | async-start | bytes 491520
  198.4 19.5 %all-to-all-start.3 = ((bf16[128,32,18]{0,2,1:T(8,128)(2,1)}), bf16[128,32,18]{0,2,1:T(8,128)(2,1)S(1)}, u32[]{:S(2)}, u32[]{:S(2)}) async-start(bf16[128,32,18]{0,2,1:T(8,128)(2,1)} %reshape.163), calls=%async_computation.4 | async-start | bytes 393216 | tf_op jit(solution)/shard_map/all_to_all | solution.py:147
Sparse Core Ops, SparseCore 0:
  121.5 50.8 reduce-scatter.4
  175.2 21.3 reduce-scatter.6
where the time goes:
time: 227 us; the launch traced here: 226 us
  blocking collectives  103 us (45%)
  waiting for transfers between devices  53.6 us (24%)
  local copies, waits for them, and re-layouts  22.6 us (10%)
  starting transfers between devices  16.4 us (7%)
  between operations  14.3 us (6%)
  matrix products  9.73 us (4%)
  other arithmetic  6.45 us (3%)
    all_to_all x1, blocking collectives, body(): lax.all_to_all(send_rows, 'ep', split_axis=0, concat_axis=0, tiled=True)  84.7 us
    unnamed x3, waiting for transfers between devices  22.2 us
    reduce_scatter x1, waiting for transfers between devices, summed_rows(): so_far = lax.psum_scatter(so_far, axis, scatter_dimension=0, tiled=True)  21 us
    all_to_all x1, blocking collectives, copy_for_each(): lax.all_to_all(jnp.broadcast_to(x[None], (peers, *x.shape)), axis, 0, 0,...  17.9 us
    all_to_all x1, waiting for transfers between devices, body(): lax.all_to_all(expert_rows.reshape(expert_rows.shape[0], experts, capacit...  9.61 us
    all_to_all x1, starting transfers between devices, body(): lax.all_to_all(expert_rows.reshape(expert_rows.shape[0], experts, capacit...  8.9 us
    gather x2, local copies, waits for them, and re-layouts, body(): picked = jnp.take(normed_b, jnp.maximum(filled - 1, 0), axis=0)  8.27 us
    unnamed x24, local copies, waits for them, and re-layouts  5.56 us
  transfers between devices with their start and end apart: 5, of which 4 were waited for; matrix products, arithmetic and copies ran while one was open for 3% of the time, Pallas kernels for 0%

commit v1 on v0

--- a/solution.py
+++ b/solution.py
@@ -117,7 +117,10 @@
     slots = slot_table(routes, experts, capacity)
     owner = jnp.arange(slots.shape[0], dtype=jnp.int32) // choices_per
     filled = jnp.zeros((experts * capacity,), jnp.int32).at[slots].set(owner + 1)
-    picked = jnp.take(normed_b, jnp.maximum(filled - 1, 0), axis=0)
+    own = lax.axis_index(TP)
+    width = normed_b.shape[1] // lax.axis_size(TP)
+    part = lax.dynamic_slice_in_dim(normed_b, own * width, width, axis=1)
+    picked = jnp.take(part, jnp.maximum(filled - 1, 0), axis=0)
     send_rows = jnp.where((filled > 0)[:, None], picked, jnp.zeros_like(picked)).reshape(
         experts, capacity, -1
     )
@@ -133,6 +136,7 @@
     arrived = lax.all_to_all(send_rows, "ep", split_axis=0, concat_axis=0, tiled=True).reshape(
         experts * capacity, -1
     )
+    arrived = lax.all_gather(arrived, TP, axis=1, tiled=True)
     gate_act = jnp.dot(arrived, gate_local, preferred_element_type=jnp.float32)
     up_act = jnp.dot(arrived, up_local, preferred_element_type=jnp.float32)
     hidden = (jax.nn.silu(gate_act) * up_act).astype(jnp.bfloat16)

time: 227 us -> 197 us (0.87)
  blocking collectives: 103 us -> 36.7 us
  waiting for transfers between devices: 53.6 us -> 101 us
  local copies, waits for them, and re-layouts: 22.6 us -> 14.1 us
  other arithmetic: 6.45 us -> 3.98 us
    all_to_all x1, blocking collectives: 84.7 us -> 23.5 us  [body(): lax.all_to_all(send_rows, 'ep', split_axis=0, concat_axis=0, tiled=True)]
    all_gather x0 -> x1, waiting for transfers between devices: none -> 41.9 us  [body(): arrived = lax.all_gather(arrived, TP, axis=1, tiled=True)]
    gather x2, local copies, waits for them, and re-layouts: 8.27 us -> 1.99 us  [body(): picked = jnp.take(part, jnp.maximum(filled - 1, 0), axis=0)]
    reduce_scatter x1, waiting for transfers between devices: 21 us -> 26.7 us  [summed_rows(): so_far = lax.psum_scatter(so_far, axis, scatter_dimension=0, tiled=True)]
    all_to_all x1, blocking collectives: 17.9 us -> 13.2 us  [copy_for_each(): lax.all_to_all(jnp.broadcast_to(x[None], (peers, *x.shape)), axis, 0, 0,...]
    unnamed x24 -> x28, local copies, waits for them, and re-layouts: 5.56 us -> 4.79 us
    unnamed x3 -> x4, waiting for transfers between devices: 22.2 us -> 21.7 us
  transfers between devices with their start and end apart: 5 -> 6, of which waited for: 4 -> 5; matrix products, arithmetic and copies ran while one was open for 3% -> 4% of each run, Pallas kernels for 0% -> 0%
where the time goes in v1:
time: 197 us; the launch traced here: 196 us
  waiting for transfers between devices  101 us (51%)
  blocking collectives  36.7 us (19%)
  starting transfers between devices  15.7 us (8%)
  local copies, waits for them, and re-layouts  14.1 us (7%)
  between operations  14.1 us (7%)
  matrix products  10.6 us (5%)
  other arithmetic  3.98 us (2%)
    all_gather x1, waiting for transfers between devices, body(): arrived = lax.all_gather(arrived, TP, axis=1, tiled=True)  41.9 us
    reduce_scatter x1, waiting for transfers between devices, summed_rows(): so_far = lax.psum_scatter(so_far, axis, scatter_dimension=0, tiled=True)  26.7 us
    all_to_all x1, blocking collectives, body(): lax.all_to_all(send_rows, 'ep', split_axis=0, concat_axis=0, tiled=True)  23.5 us
    unnamed x4, waiting for transfers between devices  21.7 us
    all_to_all x1, blocking collectives, copy_for_each(): lax.all_to_all(jnp.broadcast_to(x[None], (peers, *x.shape)), axis, 0, 0,...  13.2 us
    all_to_all x1, waiting for transfers between devices, body(): lax.all_to_all(expert_rows.reshape(expert_rows.shape[0], experts, capacit...  9.61 us
    all_to_all x1, starting transfers between devices, body(): lax.all_to_all(expert_rows.reshape(expert_rows.shape[0], experts, capacit...  8.91 us
    unnamed x28, local copies, waits for them, and re-layouts  4.79 us
  transfers between devices with their start and end apart: 6, of which 5 were waited for; matrix products, arithmetic and copies ran while one was open for 4% of the time, Pallas kernels for 0%

profile of v1, /device:TPU:1, one launch (start us, length us, event | category | flops | bytes accessed | tf_op | source)
XLA Modules:
  0.0 195.7 jit_solution(15484870692354183152)
XLA Ops:
  7.3 1.4 convert_element_type.61
  9.3 0.9 reduce-window.6
  10.9 2.9 %scatter_custom_fusion = s32[576]{0:T(1024)S(1)} fusion(s32[384]{0:T(512)S(1)} %fusion.70, s32[384]{0:T(512)S(1)} %fusion.64, s32[]{:T(128)} %constant.74.clone.1), kind=kCustom, calls=%fused_computation.130 | custom fusion | bytes 2308 | tf_op jit(solution)/shard_map/scatter | solution.py:119
  13.9 0.8 dynamic-slice
  14.8 1.9 gather_fusion
  17.3 23.5 %all_to_all.21 = bf16[32,18,128]{2,1,0:T(8,128)(2,1)S(1)} all-to-all(bf16[32,18,128]{2,1,0:T(8,128)(2,1)S(1)} %select_select_fusion), channel_id=1, replica_groups=mesh['ep'=32,'tp_0'=8,'tp_1'=2] {'ep'}, dimensions={0} | all-to-all | bytes 294912 | tf_op jit(solution)/shard_map/all_to_all | solution.py:136
  41.6 41.9 %all-gather.2.cloned.1.call-done = bf16[576,2048]{1,0:T(8,128)(2,1)} async-done(((bf16[576,128]{1,0:T(8,128)(2,1)}), bf16[576,2048]{1,0:T(8,128)(2,1)}) %all-gather.2.cloned.1.call-update) | async-done | bytes 2359312 | tf_op jit(solution)/shard_map/all_gather | solution.py:139
  83.5 3.8 %fusion.14 = f32[576,176]{0,1:T(8,128)} fusion(bf16[576,2048]{1,0:T(8,128)(2,1)} %all-gather.2.cloned.1.call-done, bf16[1,2048,176]{1,2,0:T(8,128)(2,1)} %param.25), kind=kOutput, calls=%fused_computation.26 | convolution fusion | flops 415236096 | bytes 3485696 | tf_op jit(solution)/shard_map/dot_general | solution.py:140
  87.2 4.7 %fusion = bf16[2048,576]{0,1:T(8,128)(2,1)} fusion(bf16[576,2048]{1,0:T(8,128)(2,1)S(1)} %copy-done.8, bf16[1,176,2048]{2,1,0:T(8,128)(2,1)S(1)} %copy-done, bf16[1,2048,176]{1,2,0:T(8,128)(2,1)} %param.26, f32[576,176]{0,1:T(8,128)} %fusion.14), kind=kOutput, calls=%fused_computation.3 | convolution fusion | flops 832260096 | bytes 6565888 | tf_op jit(solution)/shard_map/dot_general | solution.py:146
  92.0 1.0 copy-done.3
  94.1 2.9 %collective-permute-start = (bf16[128,30]{0,1:T(8,128)(2,1)S(1)}, bf16[128,30]{0,1:T(8,128)(2,1)S(1)}, u32[]{:S(2)}, u32[]{:S(2)}) collective-permute-start(bf16[128,30]{0,1:T(8,128)(2,1)S(1)} %slice.270), channel_id=1, source_target_pairs={{0,16},{16,32},{32,48},{48,64},{64,80},{80,96},{96,112},{112,128},... | collective-permute-start | bytes 23048 | tf_op jit(solution)/shard_map/ppermute | solution.py:14
  97.1 0.7 collective-permute-done
  98.2 13.2 %all_to_all.22 = f32[16,1,256]{2,1,0:T(1,128)S(1)} all-to-all(f32[16,1,256]{2,1,0:T(1,128)S(1)} %broadcast_in_dim.28), channel_id=1, replica_groups=mesh['ep'=32,'tp_0'=8,'tp_1'=2] {'tp_0','tp_1'}, dimensions={0} | all-to-all | bytes 32768 | tf_op jit(solution)/shard_map/all_to_all | solution.py:19
  111.8 0.9 copy.69
  112.8 3.7 %all-to-all-start.1 = ((bf16[16,128,128]{1,2,0:T(8,128)(2,1)}), bf16[16,128,128]{1,2,0:T(8,128)(2,1)S(1)}, u32[]{:S(2)}, u32[]{:S(2)}) async-start(bf16[16,128,128]{1,2,0:T(8,128)(2,1)} %bitcast.112), calls=%async_computation.1 | async-start | bytes 1048576 | tf_op jit(solution)/shard_map/all_to_all | solution.py:41
  116.5 26.7 %reduce-scatter.5.cloned.1.call-done = bf16[256,576]{0,1:T(8,128)(2,1)} async-done(((bf16[2048,576]{0,1:T(8,128)(2,1)}), bf16[256,576]{0,1:T(8,128)(2,1)}) %reduce-scatter.5.cloned.1.call-update) | async-done | bytes 294928 | tf_op jit(solution)/shard_map/reduce_scatter | solution.py:48
  143.2 1.8 copy.59
  145.2 21.6 %reduce-scatter.7.cloned.1.call-done = bf16[128,576]{1,0:T(8,128)(2,1)} async-done(((bf16[256,576]{1,0:T(8,128)(2,1)}), bf16[128,576]{1,0:T(8,128)(2,1)}) %reduce-scatter.7.cloned.1.call-update) | async-done | bytes 147472
  166.8 1.1 copy.60
  167.9 0.7 reshape.163
  168.6 8.9 %all-to-all-start.3 = ((bf16[128,32,18]{0,2,1:T(8,128)(2,1)}), bf16[128,32,18]{0,2,1:T(8,128)(2,1)S(1)}, u32[]{:S(2)}, u32[]{:S(2)}) async-start(bf16[128,32,18]{0,2,1:T(8,128)(2,1)} %reshape.163), calls=%async_computation.4 | async-start | bytes 393216 | tf_op jit(solution)/shard_map/all_to_all | solution.py:151
  177.8 0.7 copy.57
  178.6 9.6 %all-to-all-done.3 = bf16[128,32,18]{0,2,1:T(8,128)(2,1)S(1)} async-done(((bf16[128,32,18]{0,2,1:T(8,128)(2,1)}), bf16[128,32,18]{0,2,1:T(8,128)(2,1)S(1)}, u32[]{:S(2)}, u32[]{:S(2)}) %all-to-all-start.3) | async-done | bytes 147488 | tf_op jit(solution)/shard_map/all_to_all | solution.py:151
  188.2 1.0 convolution_convert_fusion.2
  (75 shorter events, 5.2 us)
Async XLA Ops:
  7.2 80.1 %copy-start = (bf16[1,176,2048]{2,1,0:T(8,128)(2,1)S(1)}, bf16[1,176,2048]{2,1,0:T(8,128)(2,1)}, u32[]{:S(2)}) copy-start(bf16[1,176,2048]{2,1,0:T(8,128)(2,1)} %param.27) | copy-start | bytes 2162692
  7.2 1.5 copy-start.1
  7.2 1.7 copy-start.6
  7.2 76.3 %all-gather.2.cloned.1.call-start = ((), (), s32[]{:S(2)}) async-start(), calls=%async_computation.6 | async-start | bytes 2506752 | tf_op jit(solution)/shard_map/all_gather | solution.py:139
  41.5 101.7 %reduce-scatter.5.cloned.1.call-start = ((), (), s32[]{:S(2)}) async-start(), calls=%async_computation.7 | async-start | bytes 2654208 | tf_op jit(solution)/shard_map/reduce_scatter | solution.py:48
  83.5 3.8 %copy-start.8 = (bf16[576,2048]{1,0:T(8,128)(2,1)S(1)}, bf16[576,2048]{1,0:T(8,128)(2,1)}, u32[]{:S(2)}) copy-start(bf16[576,2048]{1,0:T(8,128)(2,1)} %all-gather.2.cloned.1.call-done) | copy-start | bytes 7077892
  91.9 1.0 copy-start.3
  92.0 1.2 copy-start.9
  92.0 1.2 copy-start.11
  92.0 1.8 copy-start.10
  93.0 4.1 %copy-start.5 = (f32[31,128]{1,0:T(8,128)S(1)}, f32[31,128]{1,0:T(8,128)}, u32[]{:S(2)}) copy-start(f32[31,128]{1,0:T(8,128)} %param.18) | copy-start | bytes 47620
  93.2 18.2 %copy-start.2 = (bf16[128,2048]{1,0:T(8,128)(2,1)S(1)}, bf16[128,2048]{1,0:T(8,128)(2,1)}, u32[]{:S(2)}) copy-start(bf16[128,2048]{1,0:T(8,128)(2,1)} %param.20) | copy-start | bytes 1572868
  93.2 18.2 %copy-start.7 = (f32[128]{0:T(128)S(1)}, f32[128]{0:T(128)}, u32[]{:S(2)}) copy-start(f32[128]{0:T(128)} %param.19) | copy-start | bytes 1540
  94.1 3.7 %collective-permute-start = (bf16[128,30]{0,1:T(8,128)(2,1)S(1)}, bf16[128,30]{0,1:T(8,128)(2,1)S(1)}, u32[]{:S(2)}, u32[]{:S(2)}) collective-permute-start(bf16[128,30]{0,1:T(8,128)(2,1)S(1)} %slice.270), channel_id=1, source_target_pairs={{0,16},{16,32},{32,48},{48,64},{64,80},{80,96},{96,112},{112,128},... | collective-permute-start | bytes 23048 | tf_op jit(solution)/shard_map/ppermute | solution.py:14
  98.1 47.0 %copy-start.4 = (f32[192,2]{0,1:T(2,128)S(1)}, f32[192,2]{0,1:T(2,128)}, u32[]{:S(2)}) copy-start(f32[192,2]{0,1:T(2,128)} %param.24) | copy-start | bytes 4612
  112.8 55.9 %all-to-all-start.1 = ((bf16[16,128,128]{1,2,0:T(8,128)(2,1)}), bf16[16,128,128]{1,2,0:T(8,128)(2,1)S(1)}, u32[]{:S(2)}, u32[]{:S(2)}) async-start(bf16[16,128,128]{1,2,0:T(8,128)(2,1)} %bitcast.112), calls=%async_computation.1 | async-start | bytes 1048576 | tf_op jit(solution)/shard_map/all_to_all | solution.py:41
  116.5 50.3 %reduce-scatter.7.cloned.1.call-start = ((), (), s32[]{:S(2)}) async-start(), calls=%async_computation.8 | async-start | bytes 491520
  168.6 19.5 %all-to-all-start.3 = ((bf16[128,32,18]{0,2,1:T(8,128)(2,1)}), bf16[128,32,18]{0,2,1:T(8,128)(2,1)S(1)}, u32[]{:S(2)}, u32[]{:S(2)}) async-start(bf16[128,32,18]{0,2,1:T(8,128)(2,1)} %reshape.163), calls=%async_computation.4 | async-start | bytes 393216 | tf_op jit(solution)/shard_map/all_to_all | solution.py:151
Sparse Core Ops, SparseCore 0:
  41.6 41.7 all-gather.1
  92.1 51.0 reduce-scatter.4
  146.0 20.7 reduce-scatter.6

commit v2 on v0

v2 whole, which is shorter than its diff:
```python
import functools
from types import SimpleNamespace

import jax
import jax.numpy as jnp
from jax import lax
from jax.experimental import pallas as pl
from jax.experimental.pallas import tpu as pltpu
from jax.sharding import PartitionSpec as P

MESH = pl.DeviceIdType.MESH
BF = jnp.bfloat16
F32 = jnp.float32
I32 = jnp.int32
MAIN = 16
INPUTS = (
    "tok_b", "routes", "logits", "gain_b", "tok_a", "gain_a", "vw", "gw",
    "ker", "cg", "ow", "eg", "eu", "ed",
)


def iota(shape, dim):
    return lax.broadcasted_iota(I32, shape, dim)


def dot(a, b, ca=1, cb=0, precision=None):
    return lax.dot_general(
        a, b, (((ca,), (cb,)), ((), ())), precision=precision, preferred_element_type=F32
    )


def silu(v):
    return v / (1.0 + jnp.exp(-v))


def kernel(g, *refs):
    r = SimpleNamespace(**dict(zip(g.names, refs)))
    Z, X, Y, F, EX, EXT = g.Z, g.X, g.Y, g.F, g.EX, g.EXT
    NT, T, R, D, S = g.NT, g.T, g.R, g.D, g.S
    M = EX * MAIN
    HALF = M // 2
    H = Y // 2
    e = lax.axis_index("ep")
    t = lax.axis_index("tp")
    core, y = lax.rem(t, 2), lax.div(t, 2)
    z, x = lax.div(e, X), lax.rem(e, X)
    way = 1 - 2 * core
    mate = (e, t + way)
    mine = pl.ds(pl.multiple_of(core * F, F), F)

    def turn(a):
        return lax.rem(a + 4 * Y, Y)

    def tp_of(step):
        return (e, turn(y + step) * 2 + core)

    def place(b):
        i, dx = b // X, b % X
        dz = jnp.where(i % 2 == 1, (i + 1) // 2, Z - i // 2)
        return lax.rem(z + dz, Z) * X + lax.rem(x + dx, X)

    def opposite(b):
        i, dx = b // X, b % X
        back = jnp.where((i == 0) | (i == Z - 1), i, jnp.where(i % 2 == 1, i + 1, i - 1))
        return back * X + lax.rem(X - dx, X)

    def remote(src, dst, send, recv, to):
        return pltpu.make_async_remote_copy(
            src_ref=src, dst_ref=dst, send_sem=send, recv_sem=recv, device_id=to, device_id_type=MESH
        )

    barrier = pltpu.get_barrier_semaphore()

    def greet_ep(i, c):
        pl.semaphore_signal(barrier, 1, device_id=(lax.rem(e + i, EX), t), device_id_type=MESH)
        return c

    def greet_tp(i, c):
        pl.semaphore_signal(barrier, 1, device_id=(e, lax.rem(t + i, NT)), device_id_type=MESH)
        return c

    lax.fori_loop(1, EX, greet_ep, 0)
    lax.fori_loop(1, NT, greet_tp, 0)

    loads = {}
    for i, name in enumerate(INPUTS):
        loads[name] = pltpu.make_async_copy(
            getattr(r, "in_" + name), getattr(r, "v_" + name), r.in_sem.at[i]
        )
        loads[name].start()

    for name in ("tok_b", "gain_b", "routes", "logits"):
        loads[name].wait()
    squares = jnp.zeros((R, F), F32)
    for j in range(NT):
        v = r.v_tok_b[:, j * F : (j + 1) * F].astype(F32)
        squares = squares + v * v
    inv = lax.rsqrt(jnp.sum(squares, axis=1, keepdims=True) / D + 1e-6)
    own = r.v_tok_b[:, pl.ds(pl.multiple_of(t * F, F), F)].astype(F32)
    normed = (own * inv * r.v_gain_b[pl.ds(t, 1), :]).astype(BF)

    lines = iota((EX, R), 0)
    first = jnp.where(lines == r.v_routes[0:1, :], 1.0, 0.0)
    second = jnp.where(lines == r.v_routes[1:2, :], 1.0, 0.0)
    named = first + second
    earlier = jnp.where(iota((R, R), 0) < iota((R, R), 1), 1.0, 0.0).astype(BF)
    code = (named * (dot(named.astype(BF), earlier) + 1.0)).astype(BF)
    l0, l1 = r.v_logits[0:1, :], r.v_logits[1:2, :]
    top = jnp.maximum(l0, l1)
    e0, e1 = jnp.exp(l0 - top), jnp.exp(l1 - top)
    weight = first * (e0 / (e0 + e1)) + second * (e1 / (e0 + e1))
    w_hi = weight.astype(BF)
    w_lo = (weight - w_hi.astype(F32)).astype(BF)

    s = iota((S, EX), 0)
    block = jnp.where(s < M, s // MAIN, (s - M) // EXT)
    spread = jnp.where(iota((S, EX), 1) == place(block), 1.0, 0.0).astype(BF)
    q = iota((S, R), 0)
    rank = jnp.where(q < M, q % MAIN, MAIN + (q - M) % EXT) + 1
    pick = dot(spread, code) == rank.astype(F32)
    r.w_hi[...] = jnp.where(pick, dot(spread, w_hi), 0.0).astype(BF)
    r.w_lo[...] = jnp.where(pick, dot(spread, w_lo), 0.0).astype(BF)
    rows = dot(jnp.where(pick, 1.0, 0.0).astype(BF), normed)
    r.send_main[...] = rows[:M].astype(BF)
    r.ag[0, 0:MAIN, mine] = rows[:MAIN].astype(BF)
    r.rows_ext[...] = rows[M:]
    for b in range(EX):
        r.send_ext[b] = r.rows_ext[b * EXT : (b + 1) * EXT, :].astype(BF)
    r.recv_ext[0] = r.rows_ext[0:EXT, :].astype(BF)

    pl.semaphore_wait(barrier, EX - 1 + NT - 1)

    def dispatch(b, c):
        to, nb = (place(b), t), opposite(b)
        remote(
            r.send_main.at[pl.ds(pl.multiple_of(b * MAIN, MAIN), MAIN), :],
            r.ag.at[0, pl.ds(pl.multiple_of(nb * MAIN, MAIN), MAIN), mine],
            r.out_sem.at[0], r.a2a_sem.at[nb // (EX // 2)], to,
        ).start()
        remote(
            r.send_ext.at[b], r.recv_ext.at[nb], r.out_sem.at[1], r.a2a_sem.at[2], to
        ).start()
        return c

    lax.fori_loop(1, EX, dispatch, 0)

    for name in ("tok_a", "gain_a", "vw", "gw"):
        loads[name].wait()
    squares = jnp.zeros((T, F), F32)
    for j in range(NT):
        v = r.v_tok_a[:, j * F : (j + 1) * F].astype(F32)
        squares = squares + v * v
    inv = lax.rsqrt(jnp.sum(squares, axis=1, keepdims=True) / D + 1e-6)
    for j in range(NT):
        cols = slice(j * F, (j + 1) * F)
        v = r.v_tok_a[:, cols].astype(F32) * inv * r.v_gain_a[j : j + 1, :]
        r.normed_a[:, cols] = v.astype(BF)
    value = dot(r.normed_a[...], r.v_vw[...])
    gate = dot(r.normed_a[...], r.v_gw[...])
    glu = (value / (1.0 + jnp.exp(-gate))).astype(BF)
    r.padded[32:, :] = glu.astype(F32)
    r.tail[...] = glu[T - 32 :, :]
    halo = remote(r.tail, r.halo, r.out_sem.at[2], r.halo_sem, (lax.rem(e + 1, EX), t))
    halo.start()

    loads["ker"].wait()
    halo.wait_recv()
    r.padded[0:32, :] = jnp.where(e > 0, r.halo[...].astype(F32), 0.0)
    mixed = jnp.zeros((T, F), F32)
    for tap in range(g.TAPS):
        low = 32 - (g.TAPS - 1) + tap
        mixed = mixed + r.v_ker[tap : tap + 1, :] * r.padded[low : low + T, :]
    r.mixed[...] = mixed
    ones = jnp.ones((8, F), F32)
    sums = dot(ones, mixed, 1, 1, lax.Precision.HIGHEST)
    powers = dot(ones, mixed * mixed, 1, 1, lax.Precision.HIGHEST)
    r.stats[0] = jnp.where(iota((8, T), 0) == 0, sums, powers)[0:2]

    def tell(i, c):
        remote(
            r.stats.at[0], r.stats.at[NT - i], r.out_sem.at[3], r.stat_sem, (e, lax.rem(t + i, NT))
        ).start()
        return c

    lax.fori_loop(1, NT, tell, 0)

    pieces = (pl.ds(0, HALF), pl.ds(HALF, S - HALF))

    def pass_on(slot, to_slot, piece, step):
        return remote(
            r.ag.at[slot, pieces[piece], mine], r.ag.at[to_slot, pieces[piece], mine],
            r.ag_out.at[to_slot, piece], r.ag_in.at[to_slot, piece], tp_of(step),
        )

    def to_mate(slot):
        return remote(
            r.ag.at[slot, :, mine], r.ag.at[slot, :, mine], r.am_out.at[slot], r.am_in.at[slot], mate
        )

    def bulk(ref, sem):
        return pltpu.make_async_copy(ref, ref, sem)

    for piece in (0, 1):
        if piece == 0:
            bulk(r.ag.at[0, pl.ds(MAIN, HALF - MAIN), mine], r.a2a_sem.at[0]).wait()
        else:
            bulk(r.ag.at[0, pl.ds(HALF, HALF), mine], r.a2a_sem.at[1]).wait()
            bulk(r.recv_ext.at[pl.ds(1, EX - 1)], r.a2a_sem.at[2]).wait()
            for b in range(EX):
                r.rows_ext[b * EXT : (b + 1) * EXT, :] = r.recv_ext[b].astype(F32)
            r.ag[0, M:S, mine] = r.rows_ext[...].astype(BF)
        pass_on(0, turn(-way), piece, way).start()
        pass_on(0, turn(way), piece, -way).start()
    to_mate(0).start()

    loads["cg"].wait()
    loads["ow"].wait()
    bulk(r.stats.at[pl.ds(1, NT - 1)], r.stat_sem).wait()
    total = r.stats[0]
    for j in range(1, NT):
        total = total + r.stats[j]
    average = total[0:1] / g.CH
    scale = lax.rsqrt(total[1:2] / g.CH - average * average + 1e-5)
    line = iota((8, T), 0)
    both = jnp.where(line == 0, average, jnp.where(line == 1, scale, 0.0))
    line = iota((8, F), 0)
    high = lax.Precision.HIGHEST
    average = dot(both, jnp.where(line == 0, 1.0, 0.0), 0, 0, high)
    scale = dot(both, jnp.where(line == 1, 1.0, 0.0), 0, 0, high)
    act = silu((r.mixed[...] - average) * scale * r.v_cg[...]).astype(BF)
    for j in range(NT):
        r.c_part[j] = dot(act, r.v_ow[:, j * F : (j + 1) * F]).astype(BF)

    def c_mate(slot):
        return remote(
            r.c_part.at[turn(y + slot) * 2 + 1 - core], r.c_pair.at[slot],
            r.cm_out.at[slot], r.cm_in.at[slot], mate,
        )

    for slot in range(Y):
        c_mate(slot).start()

    def c_sum(slot):
        c_mate(slot).wait_recv()
        mine_part = r.c_part[turn(y + slot) * 2 + core].astype(F32)
        return mine_part + r.c_pair[slot].astype(F32)

    def c_link(slot, to_slot, step):
        return remote(
            r.c_stage.at[slot], r.c_got.at[to_slot], r.c_out.at[to_slot], r.c_in.at[to_slot], tp_of(step)
        )

    def c_step(k, sign):
        slot = turn(sign * k * way)
        last = 0 if sign > 0 else Y
        to_slot = last if k == 1 else turn(sign * (k - 1) * way)
        part = c_sum(slot)
        if k < (H if sign > 0 else H - 1):
            c_link(slot, slot, 0).wait_recv()
            part = part + r.c_got[slot].astype(F32)
        r.c_stage[slot] = part.astype(BF)
        c_link(slot, to_slot, sign * way).start()

    loads["eg"].wait()
    loads["eu"].wait()
    TILE = S // g.TILES

    def experts_in(slot, first):
        cols = pl.ds(pl.multiple_of(turn(y + slot) * 2 * F, 2 * F), 2 * F)
        wg, wu = r.v_eg[:, cols], r.v_eu[:, cols]
        for i in range(g.TILES):
            part = pl.ds(i * TILE, TILE)
            lhs = r.ag[slot, part, :]
            a, b = dot(lhs, wg, 1, 1), dot(lhs, wu, 1, 1)
            r.gate[part, :] = a if first else r.gate[part, :] + a
            r.up[part, :] = b if first else r.up[part, :] + b

    waiting = [0]
    for k in range(1, H + 1):
        for piece in (0, 1):
            down, up = turn(-k * way), turn(k * way)
            pass_on(0, down, piece, way).wait_recv()
            if k < H:
                pass_on(down, turn(-(k + 1) * way), piece, way).start()
                pass_on(0, up, piece, -way).wait_recv()
                if k < H - 1:
                    pass_on(up, turn((k + 1) * way), piece, -way).start()
        to_mate(down).start()
        if k < H:
            to_mate(up).start()
        c_step(H - k + 1, 1)
        if k > 1:
            c_step(H - k + 1, -1)
        for slot in waiting:
            to_mate(slot).wait_recv()
            experts_in(slot, k == 1)
        waiting = [down, up] if k < H else [down]
    for slot in waiting:
        to_mate(slot).wait_recv()
        experts_in(slot, False)
    r.hidden[...] = (silu(r.gate[...]) * r.up[...]).astype(BF)
    loads["ed"].wait()

    def down_cols(slot, who):
        return pl.ds(pl.multiple_of((turn(y + slot) * 2 + who) * F, F), F)

    def m_mate(slot):
        return remote(r.m_part.at[slot], r.m_pair.at[slot], r.mm_out.at[slot], r.mm_in.at[slot], mate)

    order = [turn(H * way)]
    for k in range(H - 1, 0, -1):
        order += [turn(k * way), turn(-k * way)]
    order += [0]
    for slot in order:
        r.m_part[slot] = dot(r.hidden[...], r.v_ed[:, down_cols(slot, 1 - core)]).astype(BF)
        m_mate(slot).start()

    def m_link(slot, to_slot, piece, step):
        return remote(
            r.m_stage.at[slot, pieces[piece], :], r.m_got.at[to_slot, pieces[piece], :],
            r.m_out.at[to_slot, piece], r.m_in.at[to_slot, piece], tp_of(step),
        )

    def m_step(k, sign, piece):
        slot = turn(sign * k * way)
        last = 0 if sign > 0 else Y
        to_slot = last if k == 1 else turn(sign * (k - 1) * way)
        part = pieces[piece]
        if piece == 0:
            m_mate(slot).wait_recv()
        total = dot(r.hidden[part, :], r.v_ed[:, down_cols(slot, core)])
        total = total + r.m_pair[slot, part, :].astype(F32)
        if k < (H if sign > 0 else H - 1):
            m_link(slot, slot, piece, 0).wait_recv()
            total = total + r.m_got[slot, part, :].astype(F32)
        r.m_stage[slot, part, :] = total.astype(BF)
        m_link(slot, to_slot, piece, sign * way).start()

    for k in range(H, 0, -1):
        for piece in (0, 1):
            m_step(k, 1, piece)
            if k < H:
                m_step(k, -1, piece)

    for piece in (0, 1):
        part = pieces[piece]
        if piece == 0:
            m_mate(0).wait_recv()
        total = dot(r.hidden[part, :], r.v_ed[:, down_cols(0, core)])
        total = total + r.m_pair[0, part, :].astype(F32)
        m_link(0, 0, piece, 0).wait_recv()
        total = total + r.m_got[0, part, :].astype(F32)
        m_link(0, Y, piece, 0).wait_recv()
        total = total + r.m_got[Y, part, :].astype(F32)
        r.back[part, :] = total.astype(BF)
        if piece == 1:
            r.rows_ext[...] = total[M - HALF :]
            for b in range(EX):
                r.back_ext[b] = r.rows_ext[b * EXT : (b + 1) * EXT, :].astype(BF)

        def give_back(b, c):
            to, nb = (place(b), t), opposite(b)
            remote(
                r.back.at[pl.ds(pl.multiple_of(b * MAIN, MAIN), MAIN), :],
                r.home.at[pl.ds(pl.multiple_of(nb * MAIN, MAIN), MAIN), :],
                r.out_sem.at[4], r.home_sem.at[0], to,
            ).start()
            return c

        def give_ext(b, c):
            remote(
                r.back_ext.at[b], r.home_ext.at[opposite(b)], r.out_sem.at[5], r.home_sem.at[1],
                (place(b), t),
            ).start()
            return c

        if piece == 0:
            lax.fori_loop(1, EX // 2, give_back, 0)
        else:
            lax.fori_loop(EX // 2, EX, give_back, 0)
            lax.fori_loop(1, EX, give_ext, 0)
    r.home[0:MAIN, :] = r.back[0:MAIN, :]
    r.home_ext[0] = r.back_ext[0]

    total = c_sum(0)
    c_link(0, 0, 0).wait_recv()
    total = total + r.c_got[0].astype(F32)
    c_link(0, Y, 0).wait_recv()
    total = total + r.c_got[Y].astype(F32)
    r.conv_out[...] = jnp.transpose(total).astype(BF)

    bulk(r.home.at[pl.ds(MAIN, M - MAIN), :], r.home_sem.at[0]).wait()
    bulk(r.home_ext.at[pl.ds(1, EX - 1)], r.home_sem.at[1]).wait()
    for b in range(EX):
        r.rows_ext[b * EXT : (b + 1) * EXT, :] = r.home_ext[b].astype(F32)
    r.home[M:S, :] = r.rows_ext[...].astype(BF)
    result = dot(r.home[...], r.w_hi[...], 0, 0) + dot(r.home[...], r.w_lo[...], 0, 0)
    r.moe_out[...] = result.astype(BF)

    bulk(r.send_main.at[pl.ds(MAIN, M - MAIN), :], r.out_sem.at[0]).wait()
    bulk(r.send_ext.at[pl.ds(1, EX - 1)], r.out_sem.at[1]).wait()
    halo.wait_send()
    bulk(r.stats.at[pl.ds(1, NT - 1)], r.out_sem.at[3]).wait()
    bulk(r.back.at[pl.ds(MAIN, M - MAIN), :], r.out_sem.at[4]).wait()
    bulk(r.back_ext.at[pl.ds(1, EX - 1)], r.out_sem.at[5]).wait()
    for slot in range(Y):
        to_mate(slot).wait_send()
        c_mate(slot).wait_send()
        m_mate(slot).wait_send()
    for slot in range(1, Y):
        for piece in (0, 1):
            pass_on(0, slot, piece, 0).wait_send()
    final = [0, Y] + [turn(k * way) for k in range(1, H)] + [turn(-k * way) for k in range(1, H - 1)]
    for slot in final:
        c_link(0, slot, 0).wait_send()
        for piece in (0, 1):
            m_link(0, slot, piece, 0).wait_send()


def run(Z, X, args):
    (tok_a, gain_a, vw, gw, ker, cg, ow, tok_b, gain_b, routes, logits, eg, eu, ed) = args
    EX, NT = lax.axis_size("ep"), lax.axis_size("tp")
    T, D = tok_a.shape
    R, F, HU = tok_b.shape[0], vw.shape[1], eg.shape[2]
    cap = 3 * R * routes.shape[1] // (2 * EX)
    EXT, Y = cap - MAIN, NT // 2
    S, M = EX * cap, EX * MAIN
    given = dict(
        tok_b=tok_b, routes=routes.T, logits=logits.T, gain_b=gain_b.reshape(NT, F),
        tok_a=tok_a, gain_a=gain_a.reshape(NT, F), vw=vw, gw=gw, ker=ker, cg=cg.reshape(1, F),
        ow=ow, eg=eg[0].T, eu=eu[0].T, ed=ed[0],
    )
    vm, dma = pltpu.VMEM, pltpu.SemaphoreType.DMA
    scratch = dict(
        {"v_" + n: vm(given[n].shape, given[n].dtype) for n in INPUTS},
        in_sem=dma((len(INPUTS),)), w_hi=vm((S, R), BF), w_lo=vm((S, R), BF),
        send_main=vm((M, F), BF), send_ext=vm((EX, EXT, F), BF), recv_ext=vm((EX, EXT, F), BF),
        rows_ext=vm((EX * EXT, F), F32), ag=vm((Y, S, 2 * F), BF),
        out_sem=dma((6,)), a2a_sem=dma((3,)), normed_a=vm((T, D), BF), padded=vm((T + 32, F), F32),
        tail=vm((32, F), BF), halo=vm((32, F), BF), halo_sem=dma, mixed=vm((T, F), F32),
        stats=vm((NT, 2, T), F32), stat_sem=dma,
        ag_out=dma((Y, 2)), ag_in=dma((Y, 2)), am_out=dma((Y,)), am_in=dma((Y,)),
        c_part=vm((NT, T, F), BF), c_pair=vm((Y, T, F), BF), c_stage=vm((Y, T, F), BF),
        c_got=vm((Y + 1, T, F), BF), cm_out=dma((Y,)), cm_in=dma((Y,)), c_out=dma((Y + 1,)),
        c_in=dma((Y + 1,)), gate=vm((S, HU), F32), up=vm((S, HU), F32), hidden=vm((S, HU), BF),
        m_part=vm((Y, S, F), BF), m_pair=vm((Y, S, F), BF), m_stage=vm((Y, S, F), BF),
        m_got=vm((Y + 1, S, F), BF), mm_out=dma((Y,)), mm_in=dma((Y,)), m_out=dma((Y + 1, 2)),
        m_in=dma((Y + 1, 2)), back=vm((S, F), BF), back_ext=vm((EX, EXT, F), BF),
        home=vm((S, F), BF), home_ext=vm((EX, EXT, F), BF), home_sem=dma((2,)),
    )
    names = ["in_" + n for n in INPUTS] + ["conv_out", "moe_out"] + list(scratch)
    g = SimpleNamespace(
        names=names, Z=Z, X=X, Y=Y, F=F, EX=EX, EXT=EXT, NT=NT, T=T, R=R, D=D, S=S, CH=NT * F,
        TAPS=ker.shape[0], TILES=3,
    )
    return pl.pallas_call(
        functools.partial(kernel, g),
        out_shape=(jax.ShapeDtypeStruct((F, T), BF), jax.ShapeDtypeStruct((F, R), BF)),
        in_specs=[pl.BlockSpec(memory_space=pl.ANY)] * len(INPUTS),
        out_specs=(pl.BlockSpec(memory_space=pltpu.VMEM),) * 2,
        scratch_shapes=list(scratch.values()),
        compiler_params=pltpu.CompilerParams(
            collective_id=0, has_side_effects=True, vmem_limit_bytes=60 * 1024 * 1024
        ),
    )(*[given[n] for n in INPUTS])


def solution(mesh, Z=8, X=4):
    return jax.shard_map(
        lambda *args: run(Z, X, args),
        mesh=mesh,
        in_specs=(
            P("ep", None), P(), P(None, "tp"), P(None, "tp"), P(None, "tp"), P("tp"), P("tp", None),
            P("ep", None), P(), P("ep", None), P("ep", None), P("ep", None, "tp"),
            P("ep", None, "tp"), P("ep", "tp", None),
        ),
        out_specs=(P("tp", "ep"), P("tp", "ep")),
        check_vma=False,
    )
```

time: 227 us -> 75 us (0.33)
  the two profiles are of different devices: /device:TPU:1 before, /device:TPU:14 now
where the time goes in v2:
time: 75 us; the launch traced here: 74.8 us
  Pallas kernels  72 us (96%)
  local copies, waits for them, and re-layouts  2.19 us (3%)
    pallas_call x1, Pallas kernels, run(): pl.pallas_call(functools.partial(kernel, g), out_shape=(jax.ShapeDtypeStr...  72 us
    pallas_call x1, local copies, waits for them, and re-layouts, run(): pl.pallas_call(functools.partial(kernel, g), out_shape=(jax.ShapeDtypeStr...  1.57 us

profile of v2, /device:TPU:14, one launch (start us, length us, event | category | flops | bytes accessed | tf_op | source)
XLA Modules:
  0.0 74.8 jit_solution(13044972640188253025)
XLA Ops:
  0.6 72.0 %shard_map.149 = (bf16[128,128]{1,0:T(8,128)(2,1)}, bf16[128,192]{1,0:T(8,128)(2,1)}) custom-call(bf16[192,2048]{1,0:T(8,128)(2,1)} %refs_0_.1, s32[2,192]{1,0:T(2,128)} %bitcast.17, f32[2,192]{1,0:T(2,128)} %bitcast.18, f32[16,128]{1,0:T(8,128)} %bitcast.15, bf16[128,2048]{1,0:T(8,128)(2,1)} %refs_4_.1, f32[16,128]{1,0:T(8,128)} %bitcast.16, ...), custom_call_target="tpu_custom_call" | custom-call | tf_op jit(solution)/shard_map/pallas_call | solution.py:456
  72.6 0.0 copy-start
  72.6 1.6 %copy.16 = bf16[128,192]{0,1:T(8,128)(2,1)} copy(bf16[128,192]{1,0:T(8,128)(2,1)} %get-tuple-element.3) | data formatting | bytes 98304 | tf_op jit(solution)/shard_map/pallas_call | solution.py:456
  74.2 0.0 copy-done
  74.2 0.6 copy.18
Async XLA Ops:
  72.6 1.6 %copy-start = (bf16[128,128]{1,0:T(8,128)(2,1)S(1)}, bf16[128,128]{1,0:T(8,128)(2,1)}, u32[]{:S(2)}) copy-start(bf16[128,128]{1,0:T(8,128)(2,1)} %get-tuple-element.6) | copy-start | bytes 98308

commit v3 on v2

v3 whole, which is shorter than its diff:
```python
import functools
from types import SimpleNamespace

import jax
import jax.numpy as jnp
from jax import lax
from jax.experimental import pallas as pl
from jax.experimental.pallas import tpu as pltpu
from jax.sharding import PartitionSpec as P

MESH = pl.DeviceIdType.MESH
BF = jnp.bfloat16
F32 = jnp.float32
I32 = jnp.int32
MAIN = 16
INPUTS = (
    "tok_b", "routes", "logits", "gain_b", "tok_a", "gain_a", "vw", "gw",
    "ker", "cg", "ow", "eg", "eu", "ed",
)


def iota(shape, dim):
    return lax.broadcasted_iota(I32, shape, dim)


def dot(a, b, ca=1, cb=0, precision=None):
    return lax.dot_general(
        a, b, (((ca,), (cb,)), ((), ())), precision=precision, preferred_element_type=F32
    )


def silu(v):
    return v / (1.0 + jnp.exp(-v))


def kernel(g, *refs):
    r = SimpleNamespace(**dict(zip(g.names, refs)))
    Z, X, Y, F, EX, EXT = g.Z, g.X, g.Y, g.F, g.EX, g.EXT
    NT, T, R, D, S = g.NT, g.T, g.R, g.D, g.S
    M = EX * MAIN
    HALF = M // 2
    H, DN = Y // 2, g.DN
    LA, LB = H - (DN + 1) // 2, H - 1 - DN // 2
    e = lax.axis_index("ep")
    t = lax.axis_index("tp")
    core, y = lax.rem(t, 2), lax.div(t, 2)
    z, x = lax.div(e, X), lax.rem(e, X)
    way = 1 - 2 * core
    mate = (e, t + way)
    mine = pl.ds(pl.multiple_of(core * F, F), F)
    other = pl.ds(pl.multiple_of((1 - core) * F, F), F)
    near = H - 1 + core if DN == 2 else H - DN // 2

    def turn(a):
        return lax.rem(a + 4 * Y, Y)

    def tp_of(step):
        return (e, turn(y + step) * 2 + core)

    def place(b):
        i, dx = b // X, b % X
        dz = jnp.where(i % 2 == 1, (i + 1) // 2, Z - i // 2)
        return lax.rem(z + dz, Z) * X + lax.rem(x + dx, X)

    rows_of = [lax.rem(z + i, Z) * X for i in range(Z)]
    cols_of = [lax.rem(x + i, X) for i in range(X)]

    def peer(b):
        i, dx = divmod(b, X)
        dz = ((i + 1) // 2 if i % 2 else Z - i // 2) % Z
        return (rows_of[dz] + cols_of[dx], t)

    def opposite(b):
        i, dx = divmod(b, X)
        back = i if i in (0, Z - 1) else (i + 1 if i % 2 else i - 1)
        return back * X + (X - dx) % X

    def remote(src, dst, send, recv, to):
        return pltpu.make_async_remote_copy(
            src_ref=src, dst_ref=dst, send_sem=send, recv_sem=recv, device_id=to, device_id_type=MESH
        )

    barrier = pltpu.get_barrier_semaphore()

    for b in range(EX - 1, 0, -1):
        pl.semaphore_signal(barrier, 1, device_id=peer(b), device_id_type=MESH)
    tps = [(e, lax.rem(t + i, NT)) for i in range(NT)]
    for i in range(1, NT):
        pl.semaphore_signal(barrier, 1, device_id=tps[i], device_id_type=MESH)

    loads = {}
    for i, name in enumerate(INPUTS):
        loads[name] = pltpu.make_async_copy(
            getattr(r, "in_" + name), getattr(r, "v_" + name), r.in_sem.at[i]
        )
        loads[name].start()

    for name in ("tok_b", "gain_b", "routes", "logits"):
        loads[name].wait()
    squares = jnp.zeros((R, F), F32)
    for j in range(NT):
        v = r.v_tok_b[:, j * F : (j + 1) * F].astype(F32)
        squares = squares + v * v
    inv = lax.rsqrt(jnp.sum(squares, axis=1, keepdims=True) / D + 1e-6)

    lines = iota((EX, R), 0)
    first = jnp.where(lines == r.v_routes[0:1, :], 1.0, 0.0)
    second = jnp.where(lines == r.v_routes[1:2, :], 1.0, 0.0)
    named = first + second
    earlier = jnp.where(iota((R, R), 0) < iota((R, R), 1), 1.0, 0.0).astype(BF)
    code = (named * (dot(named.astype(BF), earlier) + 1.0)).astype(BF)
    l0, l1 = r.v_logits[0:1, :], r.v_logits[1:2, :]
    top = jnp.maximum(l0, l1)
    e0, e1 = jnp.exp(l0 - top), jnp.exp(l1 - top)
    weight = first * (e0 / (e0 + e1)) + second * (e1 / (e0 + e1))
    w_hi = weight.astype(BF)
    w_lo = (weight - w_hi.astype(F32)).astype(BF)

    s = iota((S, EX), 0)
    block = jnp.where(s < M, s // MAIN, (s - M) // EXT)
    spread = jnp.where(iota((S, EX), 1) == place(block), 1.0, 0.0).astype(BF)
    q = iota((S, R), 0)
    rank = jnp.where(q < M, q % MAIN, MAIN + (q - M) % EXT) + 1
    pick = dot(spread, code) == rank.astype(F32)
    r.w_hi[...] = jnp.where(pick, dot(spread, w_hi), 0.0).astype(BF)
    r.w_lo[...] = jnp.where(pick, dot(spread, w_lo), 0.0).astype(BF)
    picks = jnp.where(pick, 1.0, 0.0).astype(BF)

    for i in range(DN + 1):
        slot = 0 if i == 0 else near + i - 1
        col = turn(y + slot) * 2 + core
        own = r.v_tok_b[:, pl.ds(pl.multiple_of(col * F, F), F)].astype(F32)
        normed = (own * inv * r.v_gain_b[pl.ds(col, 1), :]).astype(BF)
        rows = dot(picks, normed)
        r.send_main[i] = rows[:M].astype(BF)
        r.ag[slot, 0:MAIN, mine] = rows[:MAIN].astype(BF)
        r.rows_ext[...] = rows[M:]
        for b in range(EX):
            r.send_ext[i, b] = r.rows_ext[b * EXT : (b + 1) * EXT, :].astype(BF)
        r.recv_ext[i, 0] = r.rows_ext[0:EXT, :].astype(BF)

    for name in ("tok_a", "gain_a", "vw", "gw"):
        loads[name].wait()
    squares = jnp.zeros((T, F), F32)
    for j in range(NT):
        v = r.v_tok_a[:, j * F : (j + 1) * F].astype(F32)
        squares = squares + v * v
    inv = lax.rsqrt(jnp.sum(squares, axis=1, keepdims=True) / D + 1e-6)
    for j in range(NT):
        cols = slice(j * F, (j + 1) * F)
        v = r.v_tok_a[:, cols].astype(F32) * inv * r.v_gain_a[j : j + 1, :]
        r.normed_a[:, cols] = v.astype(BF)
    value = dot(r.normed_a[...], r.v_vw[...])
    gate = dot(r.normed_a[...], r.v_gw[...])
    glu = (value / (1.0 + jnp.exp(-gate))).astype(BF)
    r.padded[32:, :] = glu.astype(F32)
    r.tail[...] = glu[T - 32 :, :]
    halo = remote(r.tail, r.halo, r.out_sem.at[4], r.halo_sem, (lax.rem(e + 1, EX), t))

    pl.semaphore_wait(barrier, EX - 1 + NT - 1)

    for b in range(1, EX):
        nb = opposite(b)
        remote(
            r.send_main.at[0, pl.ds(b * MAIN, MAIN), :], r.ag.at[0, pl.ds(nb * MAIN, MAIN), mine],
            r.out_sem.at[0], r.a2a_sem.at[nb // (EX // 2)], peer(b),
        ).start()
        remote(
            r.send_ext.at[0, b], r.recv_ext.at[0, nb], r.out_sem.at[1], r.a2a_sem.at[2], peer(b)
        ).start()
    halo.start()
    for b in range(1, EX if DN else 0):
        nb = opposite(b)
        remote(
            r.send_main.at[pl.ds(1, DN), pl.ds(b * MAIN, MAIN), :],
            r.ag.at[pl.ds(near, DN), pl.ds(nb * MAIN, MAIN), mine],
            r.out_sem.at[2], r.a2a_sem.at[3], peer(b),
        ).start()
        remote(
            r.send_ext.at[pl.ds(1, DN), b], r.recv_ext.at[pl.ds(1, DN), nb],
            r.out_sem.at[3], r.a2a_sem.at[4], peer(b),
        ).start()

    cuts = [(EX * i // 4) * MAIN for i in range(4)] + [S]
    pieces = [pl.ds(a, b - a) for a, b in zip(cuts, cuts[1:])]

    def pass_on(slot, to_slot, piece, step):
        return remote(
            r.ag.at[slot, pieces[piece], mine], r.ag.at[to_slot, pieces[piece], mine],
            r.ag_out.at[to_slot, piece], r.ag_in.at[to_slot, piece], tp_of(step),
        )

    def to_mate(slot):
        return remote(
            r.ag.at[slot, :, mine], r.ag.at[slot, :, mine], r.am_out.at[slot], r.am_in.at[slot], mate
        )

    def bulk(ref, sem):
        return pltpu.make_async_copy(ref, ref, sem)

    def settle_ext(i, slot):
        for b in range(EX):
            r.rows_ext[b * EXT : (b + 1) * EXT, :] = r.recv_ext[i, b].astype(F32)
        r.ag[slot, M:S, mine] = r.rows_ext[...].astype(BF)

    bulk(r.ag.at[0, pl.ds(MAIN, HALF - MAIN), mine], r.a2a_sem.at[0]).wait()
    for piece in (0, 1):
        pass_on(0, turn(-way), piece, way).start()
        if LB:
            pass_on(0, turn(way), piece, -way).start()
    bulk(r.ag.at[0, pl.ds(HALF, HALF), mine], r.a2a_sem.at[1]).wait()
    bulk(r.recv_ext.at[0, pl.ds(1, EX - 1)], r.a2a_sem.at[2]).wait()
    settle_ext(0, 0)
    for piece in (2, 3):
        pass_on(0, turn(-way), piece, way).start()
        if LB:
            pass_on(0, turn(way), piece, -way).start()
    to_mate(0).start()

    def convolve():
        loads["ker"].wait()
        halo.wait_recv()
        r.padded[0:32, :] = jnp.where(e > 0, r.halo[...].astype(F32), 0.0)
        mixed = jnp.zeros((T, F), F32)
        for tap in range(g.TAPS):
            low = 32 - (g.TAPS - 1) + tap
            mixed = mixed + r.v_ker[tap : tap + 1, :] * r.padded[low : low + T, :]
        r.mixed[...] = mixed
        ones = jnp.ones((8, F), F32)
        sums = dot(ones, mixed, 1, 1, lax.Precision.HIGHEST)
        powers = dot(ones, mixed * mixed, 1, 1, lax.Precision.HIGHEST)
        r.stats[0] = jnp.where(iota((8, T), 0) == 0, sums, powers)[0:2]

        for i in range(1, NT):
            remote(
                r.stats.at[0], r.stats.at[NT - i], r.out_sem.at[5], r.stat_sem, tps[i]
            ).start()

    def c_mate(slot):
        return remote(
            r.c_part.at[turn(y + slot) * 2 + 1 - core], r.c_pair.at[slot],
            r.cm_out.at[slot], r.cm_in.at[slot], mate,
        )

    def channel_norm():
        loads["cg"].wait()
        loads["ow"].wait()
        bulk(r.stats.at[pl.ds(1, NT - 1)], r.stat_sem).wait()
        total = r.stats[0]
        for j in range(1, NT):
            total = total + r.stats[j]
        average = total[0:1] / g.CH
        scale = lax.rsqrt(total[1:2] / g.CH - average * average + 1e-5)
        line = iota((8, T), 0)
        both = jnp.where(line == 0, average, jnp.where(line == 1, scale, 0.0))
        line = iota((8, F), 0)
        high = lax.Precision.HIGHEST
        average = dot(both, jnp.where(line == 0, 1.0, 0.0), 0, 0, high)
        scale = dot(both, jnp.where(line == 1, 1.0, 0.0), 0, 0, high)
        act = silu((r.mixed[...] - average) * scale * r.v_cg[...]).astype(BF)
        for j in range(NT):
            r.c_part[j] = dot(act, r.v_ow[:, j * F : (j + 1) * F]).astype(BF)
        for slot in range(Y):
            c_mate(slot).start()

    def c_sum(slot):
        c_mate(slot).wait_recv()
        mine_part = r.c_part[turn(y + slot) * 2 + core].astype(F32)
        return mine_part + r.c_pair[slot].astype(F32)

    def c_link(slot, to_slot, step):
        return remote(
            r.c_stage.at[slot], r.c_got.at[to_slot], r.c_out.at[to_slot], r.c_in.at[to_slot], tp_of(step)
        )

    def c_step(k, sign):
        slot = turn(sign * k * way)
        last = 0 if sign > 0 else Y
        to_slot = last if k == 1 else turn(sign * (k - 1) * way)
        part = c_sum(slot)
        if k < (H if sign > 0 else H - 1):
            c_link(slot, slot, 0).wait_recv()
            part = part + r.c_got[slot].astype(F32)
        r.c_stage[slot] = part.astype(BF)
        c_link(slot, to_slot, sign * way).start()

    def c_both(k):
        c_step(k, 1)
        if k < H:
            c_step(k, -1)

    TILE = S // g.TILES

    def experts_in(slot, first):
        to_mate(slot).wait_recv()
        cols = pl.ds(pl.multiple_of(turn(y + slot) * 2 * F, 2 * F), 2 * F)
        wg, wu = r.v_eg[:, cols], r.v_eu[:, cols]
        for i in range(g.TILES):
            part = pl.ds(i * TILE, TILE)
            lhs = r.ag[slot, part, :]
            a, b = dot(lhs, wg, 1, 1), dot(lhs, wu, 1, 1)
            r.gate[part, :] = a if first else r.gate[part, :] + a
            r.up[part, :] = b if first else r.up[part, :] + b

    steps = list(range(H, 0, -1))
    waiting = [0]
    for k in range(1, LA + 1):
        down, up = turn(-k * way), turn(k * way)
        for piece in range(4):
            pass_on(0, down, piece, way).wait_recv()
            if k < LA:
                pass_on(down, turn(-(k + 1) * way), piece, way).start()
            if k <= LB:
                pass_on(0, up, piece, -way).wait_recv()
                if k < LB:
                    pass_on(up, turn((k + 1) * way), piece, -way).start()
        to_mate(down).start()
        if k <= LB:
            to_mate(up).start()
        if k == 1:
            loads["eg"].wait()
            loads["eu"].wait()
        for slot in waiting:
            experts_in(slot, k == 1)
        waiting = [down, up] if k <= LB else [down]
        if k == 1:
            convolve()
        elif k == 2:
            channel_norm()
        else:
            c_both(steps.pop(0))
    if LA < 2:
        if LA < 1:
            convolve()
        channel_norm()
    if DN:
        bulk(r.ag.at[pl.ds(near, DN), pl.ds(MAIN, M - MAIN), mine], r.a2a_sem.at[3]).wait()
        bulk(r.recv_ext.at[pl.ds(1, DN), pl.ds(1, EX - 1)], r.a2a_sem.at[4]).wait()
        for i in range(DN):
            settle_ext(1 + i, near + i)
            to_mate(near + i).start()
        for slot in waiting:
            experts_in(slot, False)
        waiting = [near + i for i in range(DN)]
    for slot in waiting:
        experts_in(slot, False)
    r.hidden[...] = (silu(r.gate[...]) * r.up[...]).astype(BF)
    loads["ed"].wait()

    def m_mate(slot, piece):
        part = slice(None) if piece is None else pieces[piece]
        n = 0 if piece is None else piece
        return remote(
            r.m_full.at[slot, part, other], r.m_pair.at[slot, part, :],
            r.mm_out.at[slot, n], r.mm_in.at[slot, n], mate,
        )

    def produce(slot):
        cols = pl.ds(pl.multiple_of(turn(y + slot) * 2 * F, 2 * F), 2 * F)
        r.m_full[slot] = dot(r.hidden[...], r.v_ed[:, cols]).astype(BF)
        m_mate(slot, None).start()

    def m_link(slot, to_slot, piece, step):
        return remote(
            r.m_stage.at[slot, pieces[piece], :], r.m_got.at[to_slot, pieces[piece], :],
            r.m_out.at[to_slot, piece], r.m_in.at[to_slot, piece], tp_of(step),
        )

    def pair_sum(slot, piece):
        part = pieces[piece]
        return r.m_full[slot, part, mine].astype(F32) + r.m_pair[slot, part, :].astype(F32)

    def m_step(k, sign, piece):
        slot = turn(sign * k * way)
        last = 0 if sign > 0 else Y
        to_slot = last if k == 1 else turn(sign * (k - 1) * way)
        part = pieces[piece]
        total = pair_sum(slot, piece)
        if k < (H if sign > 0 else H - 1):
            m_link(slot, slot, piece, 0).wait_recv()
            total = total + r.m_got[slot, part, :].astype(F32)
        r.m_stage[slot, part, :] = total.astype(BF)
        m_link(slot, to_slot, piece, sign * way).start()

    far = H
    cols = pl.ds(pl.multiple_of(turn(y + far) * 2 * F, 2 * F), 2 * F)
    for piece in (3, 2, 1, 0):
        part = pieces[piece]
        r.m_full[far, part, :] = dot(r.hidden[part, :], r.v_ed[:, cols]).astype(BF)
        m_mate(far, piece).start()
    for k in range(H - 1, 0, -1):
        if k == H - 1:
            for slot in (turn(-k * way), turn(k * way)):
                produce(slot)
            for piece in (3, 2, 1, 0):
                m_mate(far, piece).wait_recv()
                m_step(H, 1, piece)
            while len(steps) > 2:
                c_both(steps.pop(0))
        m_mate(turn(-k * way), None).wait_recv()
        if k == H - 1:
            for piece in (3, 2, 1, 0):
                m_step(k, -1, piece)
        for slot in (turn(-(k - 1) * way), turn((k - 1) * way)) if k > 1 else (0,):
            produce(slot)
        if k < H - 1 and steps:
            c_both(steps.pop(0))
        m_mate(turn(k * way), None).wait_recv()
        for piece in (3, 2, 1, 0):
            m_step(k, 1, piece)
            if k < H - 1:
                m_step(k, -1, piece)

    m_mate(0, None).wait_recv()
    for piece in (3, 2, 1, 0):
        part = pieces[piece]
        total = pair_sum(0, piece)
        m_link(0, 0, piece, 0).wait_recv()
        total = total + r.m_got[0, part, :].astype(F32)
        m_link(0, Y, piece, 0).wait_recv()
        total = total + r.m_got[Y, part, :].astype(F32)
        r.back[part, :] = total.astype(BF)
        if piece == 3:
            r.rows_ext[...] = total[M - cuts[3] :]
            for b in range(EX):
                r.back_ext[b] = r.rows_ext[b * EXT : (b + 1) * EXT, :].astype(BF)
            for b in range(EX - 1, 0, -1):
                remote(
                    r.back_ext.at[b], r.home_ext.at[opposite(b)],
                    r.out_sem.at[7], r.home_sem.at[1], peer(b),
                ).start()
        for b in range(EX * (piece + 1) // 4 - 1, max(EX * piece // 4, 1) - 1, -1):
            remote(
                r.back.at[pl.ds(b * MAIN, MAIN), :], r.home.at[pl.ds(opposite(b) * MAIN, MAIN), :],
                r.out_sem.at[6], r.home_sem.at[0], peer(b),
            ).start()
    r.home[0:MAIN, :] = r.back[0:MAIN, :]
    r.home_ext[0] = r.back_ext[0]

    while steps:
        c_both(steps.pop(0))
    total = c_sum(0)
    c_link(0, 0, 0).wait_recv()
    total = total + r.c_got[0].astype(F32)
    c_link(0, Y, 0).wait_recv()
    total = total + r.c_got[Y].astype(F32)
    r.conv_out[...] = jnp.transpose(total).astype(BF)

    bulk(r.home_ext.at[pl.ds(1, EX - 1)], r.home_sem.at[1]).wait()
    for b in range(EX):
        r.rows_ext[b * EXT : (b + 1) * EXT, :] = r.home_ext[b].astype(F32)
    r.home[M:S, :] = r.rows_ext[...].astype(BF)
    bulk(r.home.at[pl.ds(MAIN, M - MAIN), :], r.home_sem.at[0]).wait()
    result = dot(r.w_hi[...], r.home[...], 0, 0) + dot(r.w_lo[...], r.home[...], 0, 0)
    r.moe_out[...] = result.astype(BF)

    bulk(r.send_main.at[0, pl.ds(MAIN, M - MAIN), :], r.out_sem.at[0]).wait()
    bulk(r.send_ext.at[0, pl.ds(1, EX - 1)], r.out_sem.at[1]).wait()
    if DN:
        bulk(r.send_main.at[pl.ds(1, DN), pl.ds(MAIN, M - MAIN), :], r.out_sem.at[2]).wait()
        bulk(r.send_ext.at[pl.ds(1, DN), pl.ds(1, EX - 1)], r.out_sem.at[3]).wait()
    halo.wait_send()
    bulk(r.stats.at[pl.ds(1, NT - 1)], r.out_sem.at[5]).wait()
    bulk(r.back.at[pl.ds(MAIN, M - MAIN), :], r.out_sem.at[6]).wait()
    bulk(r.back_ext.at[pl.ds(1, EX - 1)], r.out_sem.at[7]).wait()
    for slot in range(Y):
        to_mate(slot).wait_send()
        c_mate(slot).wait_send()
        if slot == far:
            for piece in range(4):
                m_mate(slot, piece).wait_send()
        else:
            m_mate(slot, None).wait_send()
    passed = [turn(-k * way) for k in range(1, LA + 1)] + [turn(k * way) for k in range(1, LB + 1)]
    for slot in passed:
        for piece in range(4):
            pass_on(0, slot, piece, 0).wait_send()
    final = [0, Y] + [turn(k * way) for k in range(1, H)] + [turn(-k * way) for k in range(1, H - 1)]
    for slot in final:
        c_link(0, slot, 0).wait_send()
        for piece in range(4):
            m_link(0, slot, piece, 0).wait_send()


def run(Z, X, args):
    (tok_a, gain_a, vw, gw, ker, cg, ow, tok_b, gain_b, routes, logits, eg, eu, ed) = args
    EX, NT = lax.axis_size("ep"), lax.axis_size("tp")
    T, D = tok_a.shape
    R, F, HU = tok_b.shape[0], vw.shape[1], eg.shape[2]
    cap = 3 * R * routes.shape[1] // (2 * EX)
    EXT, Y, DN = cap - MAIN, NT // 2, 2
    S, M = EX * cap, EX * MAIN
    given = dict(
        tok_b=tok_b, routes=routes.T, logits=logits.T, gain_b=gain_b.reshape(NT, F),
        tok_a=tok_a, gain_a=gain_a.reshape(NT, F), vw=vw, gw=gw, ker=ker, cg=cg.reshape(1, F),
        ow=ow, eg=eg[0].T, eu=eu[0].T, ed=ed[0],
    )
    vm, dma = pltpu.VMEM, pltpu.SemaphoreType.DMA
    scratch = dict(
        {"v_" + n: vm(given[n].shape, given[n].dtype) for n in INPUTS},
        in_sem=dma((len(INPUTS),)), w_hi=vm((S, R), BF), w_lo=vm((S, R), BF),
        send_main=vm((DN + 1, M, F), BF), send_ext=vm((DN + 1, EX, EXT, F), BF),
        recv_ext=vm((DN + 1, EX, EXT, F), BF),
        rows_ext=vm((EX * EXT, F), F32), ag=vm((Y, S, 2 * F), BF),
        out_sem=dma((8,)), a2a_sem=dma((5,)), normed_a=vm((T, D), BF), padded=vm((T + 32, F), F32),
        tail=vm((32, F), BF), halo=vm((32, F), BF), halo_sem=dma, mixed=vm((T, F), F32),
        stats=vm((NT, 2, T), F32), stat_sem=dma,
        ag_out=dma((Y, 4)), ag_in=dma((Y, 4)), am_out=dma((Y,)), am_in=dma((Y,)),
        c_part=vm((NT, T, F), BF), c_pair=vm((Y, T, F), BF), c_stage=vm((Y, T, F), BF),
        c_got=vm((Y + 1, T, F), BF), cm_out=dma((Y,)), cm_in=dma((Y,)), c_out=dma((Y + 1,)),
        c_in=dma((Y + 1,)), gate=vm((S, HU), F32), up=vm((S, HU), F32), hidden=vm((S, HU), BF),
        m_full=vm((Y, S, 2 * F), BF), m_pair=vm((Y, S, F), BF), m_stage=vm((Y, S, F), BF),
        m_got=vm((Y + 1, S, F), BF), mm_out=dma((Y, 4)), mm_in=dma((Y, 4)), m_out=dma((Y + 1, 4)),
        m_in=dma((Y + 1, 4)), back=vm((S, F), BF), back_ext=vm((EX, EXT, F), BF),
        home=vm((S, F), BF), home_ext=vm((EX, EXT, F), BF), home_sem=dma((2,)),
    )
    names = ["in_" + n for n in INPUTS] + ["conv_out", "moe_out"] + list(scratch)
    g = SimpleNamespace(
        names=names, Z=Z, X=X, Y=Y, F=F, EX=EX, EXT=EXT, NT=NT, T=T, R=R, D=D, S=S, CH=NT * F,
        TAPS=ker.shape[0], TILES=3, DN=DN,
    )
    conv_out, moe_out = pl.pallas_call(
        functools.partial(kernel, g),
        out_shape=(pltpu.VMEM((F, T), BF), pltpu.VMEM((R, F), BF)),
        in_specs=[pl.BlockSpec(memory_space=pl.ANY)] * len(INPUTS),
        out_specs=(pl.BlockSpec(memory_space=pltpu.VMEM),) * 2,
        scratch_shapes=list(scratch.values()),
        compiler_params=pltpu.CompilerParams(
            collective_id=0, has_side_effects=True, vmem_limit_bytes=60 * 1024 * 1024
        ),
    )(*[given[n] for n in INPUTS])
    return conv_out, moe_out.T


def solution(mesh, Z=8, X=4):
    return jax.shard_map(
        lambda *args: run(Z, X, args),
        mesh=mesh,
        in_specs=(
            P("ep", None), P(), P(None, "tp"), P(None, "tp"), P(None, "tp"), P("tp"), P("tp", None),
            P("ep", None), P(), P("ep", None), P("ep", None), P("ep", None, "tp"),
            P("ep", None, "tp"), P("ep", "tp", None),
        ),
        out_specs=(P("tp", "ep"), P("tp", "ep")),
        check_vma=False,
    )
```

time: 75 us -> 66 us (0.88)
  the two profiles are of different devices: /device:TPU:14 before, /device:TPU:1 now
where the time goes in v3:
time: 66 us; the launch traced here: 65.9 us
  Pallas kernels  64 us (97%)
  local copies, waits for them, and re-layouts  1.24 us (2%)
    pallas_call x1, Pallas kernels, run(): pl.pallas_call(functools.partial(kernel, g), out_shape=(pltpu.VMEM((F, T)...  64 us

profile of v3, /device:TPU:1, one launch (start us, length us, event | category | flops | bytes accessed | tf_op | source)
XLA Modules:
  0.0 65.9 jit_solution(11665182222761347273)
XLA Ops:
  0.6 64.0 %shard_map.149 = (bf16[128,128]{1,0:T(8,128)(2,1)S(1)}, bf16[192,128]{1,0:T(8,128)(2,1)S(1)}) custom-call(bf16[192,2048]{1,0:T(8,128)(2,1)} %refs_0_.1, s32[2,192]{1,0:T(2,128)} %bitcast.19, f32[2,192]{1,0:T(2,128)} %bitcast.20, f32[16,128]{1,0:T(8,128)} %bitcast.17, bf16[128,2048]{1,0:T(8,128)(2,1)} %refs_4_.1, f32[16,128]{1,0:T(8,128)} %bitcast.18, ...), custom_call_target="tpu_custom_call" | custom-call | tf_op jit(solution)/shard_map/pallas_call | solution.py:522
  64.6 0.6 copy.18
  65.3 0.6 copy.19

commit v4 on v3

v4 whole, which is shorter than its diff:
```python
import functools
from types import SimpleNamespace

import jax
import jax.numpy as jnp
from jax import lax
from jax.experimental import pallas as pl
from jax.experimental.pallas import tpu as pltpu
from jax.sharding import PartitionSpec as P

MESH = pl.DeviceIdType.MESH
BF = jnp.bfloat16
F32 = jnp.float32
I32 = jnp.int32
MAIN = 16
INPUTS = (
    "routes", "logits", "tok_b", "gain_b", "tok_a", "gain_a", "vw", "gw",
    "ker", "cg", "ow", "eg", "eu", "ed",
)


def iota(shape, dim):
    return lax.broadcasted_iota(I32, shape, dim)


def dot(a, b, ca=1, cb=0, precision=None):
    return lax.dot_general(
        a, b, (((ca,), (cb,)), ((), ())), precision=precision, preferred_element_type=F32
    )


def silu(v):
    return v / (1.0 + jnp.exp(-v))


def kernel(g, *refs):
    r = SimpleNamespace(**dict(zip(g.names, refs)))
    Z, X, Y, F, EX, EXT = g.Z, g.X, g.Y, g.F, g.EX, g.EXT
    NT, T, R, D, S = g.NT, g.T, g.R, g.D, g.S
    M = EX * MAIN
    HALF = M // 2
    H, DN = Y // 2, g.DN
    LA, LB = H - (DN + 1) // 2, H - 1 - DN // 2
    e = lax.axis_index("ep")
    t = lax.axis_index("tp")
    core, y = lax.rem(t, 2), lax.div(t, 2)
    z, x = lax.div(e, X), lax.rem(e, X)
    way = 1 - 2 * core
    mate = (e, t + way)
    mine = pl.ds(pl.multiple_of(core * F, F), F)
    other = pl.ds(pl.multiple_of((1 - core) * F, F), F)
    near = H - 1 + core if DN == 2 else H - DN // 2

    def turn(a):
        return lax.rem(a + 4 * Y, Y)

    def tp_of(step):
        return (e, turn(y + step) * 2 + core)

    def place(b):
        i, dx = b // X, b % X
        dz = jnp.where(i % 2 == 1, (i + 1) // 2, Z - i // 2)
        return lax.rem(z + dz, Z) * X + lax.rem(x + dx, X)

    rows_of = [lax.rem(z + i, Z) * X for i in range(Z)]
    cols_of = [lax.rem(x + i, X) for i in range(X)]

    def peer(b):
        i, dx = divmod(b, X)
        dz = ((i + 1) // 2 if i % 2 else Z - i // 2) % Z
        return (rows_of[dz] + cols_of[dx], t)

    def opposite(b):
        i, dx = divmod(b, X)
        back = i if i in (0, Z - 1) else (i + 1 if i % 2 else i - 1)
        return back * X + (X - dx) % X

    def remote(src, dst, send, recv, to):
        return pltpu.make_async_remote_copy(
            src_ref=src, dst_ref=dst, send_sem=send, recv_sem=recv, device_id=to, device_id_type=MESH
        )

    loads = {}
    for i, name in enumerate(INPUTS):
        loads[name] = pltpu.make_async_copy(
            getattr(r, "in_" + name), getattr(r, "v_" + name), r.in_sem.at[i]
        )
    for name in INPUTS[:4]:
        loads[name].start()

    barrier = pltpu.get_barrier_semaphore()

    for b in range(EX - 1, 0, -1):
        pl.semaphore_signal(barrier, 1, device_id=peer(b), device_id_type=MESH)
    tps = [(e, lax.rem(t + i, NT)) for i in range(NT)]
    for i in range(1, NT):
        pl.semaphore_signal(barrier, 1, device_id=tps[i], device_id_type=MESH)
    for name in INPUTS[4:]:
        loads[name].start()

    s = iota((1, S), 1)
    block = jnp.where(s < M, s // MAIN, (s - M) // EXT)
    rank = jnp.where(s < M, s % MAIN, MAIN + (s - M) % EXT) + 1
    line = iota((EX + 8, S), 0)
    spread = jnp.where(line == place(block), 1.0, jnp.where(line == EX, rank.astype(F32), 0.0))
    r.spread[...] = spread.astype(BF)
    for name in ("routes", "logits"):
        loads[name].wait()
    lines = iota((EX, R), 0)
    first = jnp.where(lines == r.v_routes[0:1, :], 1.0, 0.0)
    second = jnp.where(lines == r.v_routes[1:2, :], 1.0, 0.0)
    named = first + second
    earlier = jnp.where(iota((R, R), 0) < iota((R, R), 1), 1.0, 0.0).astype(BF)
    r.code[0:EX, :] = named * (dot(named.astype(BF), earlier) + 1.0)
    r.code[EX:, :] = jnp.where(iota((8, R), 0) == 0, -1.0, 0.0)
    l0, l1 = r.v_logits[0:1, :], r.v_logits[1:2, :]
    top = jnp.maximum(l0, l1)
    e0, e1 = jnp.exp(l0 - top), jnp.exp(l1 - top)
    weight = first * (e0 / (e0 + e1)) + second * (e1 / (e0 + e1))
    r.weight[...] = weight

    for name in ("tok_b", "gain_b"):
        loads[name].wait()
    squares = jnp.zeros((R, F), F32)
    for j in range(NT):
        v = r.v_tok_b[:, j * F : (j + 1) * F].astype(F32)
        squares = squares + v * v
    inv = lax.rsqrt(jnp.sum(squares, axis=1, keepdims=True) / D + 1e-6)

    lag = dot(r.spread[...], r.code[...].astype(BF), 0, 0)
    r.picks[...] = jnp.where(lag == 0.0, 1.0, 0.0).astype(BF)

    def rows_for(i, slot):
        col = turn(y + slot) * 2 + core
        own = r.v_tok_b[:, pl.ds(pl.multiple_of(col * F, F), F)].astype(F32)
        normed = (own * inv * r.v_gain_b[pl.ds(col, 1), :]).astype(BF)
        rows = dot(r.picks[...], normed)
        r.send_main[i] = rows[:M].astype(BF)
        r.ag[slot, 0:MAIN, mine] = rows[:MAIN].astype(BF)
        r.rows_ext[...] = rows[M:]
        for b in range(EX):
            r.send_ext[i, b] = r.rows_ext[b * EXT : (b + 1) * EXT, :].astype(BF)
        r.recv_ext[i, 0] = r.rows_ext[0:EXT, :].astype(BF)

    rows_for(0, 0)
    pl.semaphore_wait(barrier, EX - 1 + NT - 1)
    for b in range(1, EX):
        nb = opposite(b)
        remote(
            r.send_main.at[0, pl.ds(b * MAIN, MAIN), :], r.ag.at[0, pl.ds(nb * MAIN, MAIN), mine],
            r.out_sem.at[0], r.a2a_sem.at[nb // (EX // 2)], peer(b),
        ).start()
        remote(
            r.send_ext.at[0, b], r.recv_ext.at[0, nb], r.out_sem.at[1], r.a2a_sem.at[2], peer(b)
        ).start()

    for name in ("tok_a", "gain_a", "vw", "gw"):
        loads[name].wait()
    squares = jnp.zeros((T, F), F32)
    for j in range(NT):
        v = r.v_tok_a[:, j * F : (j + 1) * F].astype(F32)
        squares = squares + v * v
    inv_a = lax.rsqrt(jnp.sum(squares, axis=1, keepdims=True) / D + 1e-6)
    for j in range(NT):
        cols = slice(j * F, (j + 1) * F)
        v = r.v_tok_a[:, cols].astype(F32) * inv_a * r.v_gain_a[j : j + 1, :]
        r.normed_a[:, cols] = v.astype(BF)
    value = dot(r.normed_a[...], r.v_vw[...])
    gate = dot(r.normed_a[...], r.v_gw[...])
    glu = (value / (1.0 + jnp.exp(-gate))).astype(BF)
    r.padded[32:, :] = glu.astype(F32)
    r.tail[...] = glu[T - 32 :, :]
    halo = remote(r.tail, r.halo, r.out_sem.at[4], r.halo_sem, (lax.rem(e + 1, EX), t))
    halo.start()

    for i in range(DN):
        rows_for(1 + i, near + i)
    for b in range(1, EX if DN else 0):
        nb = opposite(b)
        remote(
            r.send_main.at[pl.ds(1, DN), pl.ds(b * MAIN, MAIN), :],
            r.ag.at[pl.ds(near, DN), pl.ds(nb * MAIN, MAIN), mine],
            r.out_sem.at[2], r.a2a_sem.at[3], peer(b),
        ).start()
        remote(
            r.send_ext.at[pl.ds(1, DN), b], r.recv_ext.at[pl.ds(1, DN), nb],
            r.out_sem.at[3], r.a2a_sem.at[4], peer(b),
        ).start()
    weight = r.weight[...]
    w_hi = weight.astype(BF)
    w_lo = (weight - w_hi.astype(F32)).astype(BF)
    r.w_hi[...] = (r.picks[...].astype(F32) * dot(r.spread[0:EX, :], w_hi, 0, 0)).astype(BF)
    r.w_lo[...] = (r.picks[...].astype(F32) * dot(r.spread[0:EX, :], w_lo, 0, 0)).astype(BF)

    cuts = [(EX * i // 4) * MAIN for i in range(4)] + [S]
    pieces = [pl.ds(a, b - a) for a, b in zip(cuts, cuts[1:])]

    def pass_on(sign, k, piece):
        return remote(
            r.ag.at[turn(-sign * (k - 1) * way), pieces[piece], mine],
            r.ag.at[turn(-sign * k * way), pieces[piece], mine],
            r.out_sem.at[8], r.ag_in.at[k - 1 if sign > 0 else LA + k - 1, piece], tp_of(sign * way),
        )

    def to_mate(slot):
        return remote(
            r.ag.at[slot, :, mine], r.ag.at[slot, :, mine], r.out_sem.at[9], r.am_in.at[slot], mate
        )

    def bulk(ref, sem):
        return pltpu.make_async_copy(ref, ref, sem)

    def settle_ext(i, slot):
        for b in range(EX):
            r.rows_ext[b * EXT : (b + 1) * EXT, :] = r.recv_ext[i, b].astype(F32)
        r.ag[slot, M:S, mine] = r.rows_ext[...].astype(BF)

    def convolve():
        loads["ker"].wait()
        halo.wait_recv()
        r.padded[0:32, :] = jnp.where(e > 0, r.halo[...].astype(F32), 0.0)
        mixed = jnp.zeros((T, F), F32)
        for tap in range(g.TAPS):
            low = 32 - (g.TAPS - 1) + tap
            mixed = mixed + r.v_ker[tap : tap + 1, :] * r.padded[low : low + T, :]
        r.mixed[...] = mixed
        ones = jnp.ones((8, F), F32)
        sums = dot(ones, mixed, 1, 1, lax.Precision.HIGHEST)
        powers = dot(ones, mixed * mixed, 1, 1, lax.Precision.HIGHEST)
        r.stats[0] = jnp.where(iota((8, T), 0) == 0, sums, powers)[0:2]

        for i in range(1, NT):
            remote(
                r.stats.at[0], r.stats.at[NT - i], r.out_sem.at[5], r.stat_sem, tps[i]
            ).start()

    bulk(r.ag.at[0, pl.ds(MAIN, HALF - MAIN), mine], r.a2a_sem.at[0]).wait()
    for piece in (0, 1):
        if LA:
            pass_on(1, 1, piece).start()
        if LB:
            pass_on(-1, 1, piece).start()
    convolve()
    bulk(r.ag.at[0, pl.ds(HALF, HALF), mine], r.a2a_sem.at[1]).wait()
    bulk(r.recv_ext.at[0, pl.ds(1, EX - 1)], r.a2a_sem.at[2]).wait()
    settle_ext(0, 0)
    for piece in (2, 3):
        if LA:
            pass_on(1, 1, piece).start()
        if LB:
            pass_on(-1, 1, piece).start()
    to_mate(0).start()

    def c_mate(slot):
        return remote(
            r.c_part.at[turn(y + slot) * 2 + 1 - core], r.c_pair.at[slot],
            r.out_sem.at[10], r.cm_in, mate,
        )

    def channel_norm():
        loads["cg"].wait()
        loads["ow"].wait()
        bulk(r.stats.at[pl.ds(1, NT - 1)], r.stat_sem).wait()
        total = r.stats[0]
        for j in range(1, NT):
            total = total + r.stats[j]
        average = total[0:1] / g.CH
        scale = lax.rsqrt(total[1:2] / g.CH - average * average + 1e-5)
        line = iota((8, T), 0)
        both = jnp.where(line == 0, average, jnp.where(line == 1, scale, 0.0))
        line = iota((8, F), 0)
        high = lax.Precision.HIGHEST
        average = dot(both, jnp.where(line == 0, 1.0, 0.0), 0, 0, high)
        scale = dot(both, jnp.where(line == 1, 1.0, 0.0), 0, 0, high)
        act = silu((r.mixed[...] - average) * scale * r.v_cg[...]).astype(BF)
        for j in range(NT):
            r.c_part[j] = dot(act, r.v_ow[:, j * F : (j + 1) * F]).astype(BF)
        for slot in range(Y):
            c_mate(slot).start()

    def c_sum(slot):
        mine_part = r.c_part[turn(y + slot) * 2 + core].astype(F32)
        return mine_part + r.c_pair[slot].astype(F32)

    def hop(k, sign):
        return H - k if sign > 0 else 2 * H - 1 - k

    def c_link(k, sign):
        n = hop(k, sign)
        return remote(
            r.c_stage.at[n], r.c_got.at[n], r.out_sem.at[11], r.c_in.at[n], tp_of(sign * way)
        )

    def c_step(k, sign):
        part = c_sum(turn(sign * k * way))
        if k < (H if sign > 0 else H - 1):
            c_link(k + 1, sign).wait_recv()
            part = part + r.c_got[hop(k + 1, sign)].astype(F32)
        r.c_stage[hop(k, sign)] = part.astype(BF)
        c_link(k, sign).start()

    def c_both(k):
        if k == H:
            bulk(r.c_pair, r.cm_in).wait()
        c_step(k, 1)
        if k < H:
            c_step(k, -1)

    TILE = S // g.TILES

    def experts_in(slot, first):
        to_mate(slot).wait_recv()
        cols = pl.ds(pl.multiple_of(turn(y + slot) * 2 * F, 2 * F), 2 * F)
        wg, wu = r.v_eg[:, cols], r.v_eu[:, cols]
        for i in range(g.TILES):
            part = pl.ds(i * TILE, TILE)
            lhs = r.ag[slot, part, :]
            a, b = dot(lhs, wg, 1, 1), dot(lhs, wu, 1, 1)
            r.gate[part, :] = a if first else r.gate[part, :] + a
            r.up[part, :] = b if first else r.up[part, :] + b

    loads["eg"].wait()
    loads["eu"].wait()
    steps = list(range(H, 0, -1))
    waiting = [0]

    def take_direct():
        bulk(r.ag.at[pl.ds(near, DN), pl.ds(MAIN, M - MAIN), mine], r.a2a_sem.at[3]).wait()
        bulk(r.recv_ext.at[pl.ds(1, DN), pl.ds(1, EX - 1)], r.a2a_sem.at[4]).wait()
        for i in range(DN):
            settle_ext(1 + i, near + i)
            to_mate(near + i).start()
        return [H] if DN == 2 else [near + i for i in range(DN)]

    for k in range(1, LA + 1):
        if DN and k == g.DIRECT_AT:
            waiting = waiting + take_direct()
        down, up = turn(-k * way), turn(k * way)
        for piece in range(4):
            pass_on(1, k, piece).wait_recv()
            if k < LA:
                pass_on(1, k + 1, piece).start()
            if k <= LB:
                pass_on(-1, k, piece).wait_recv()
                if k < LB:
                    pass_on(-1, k + 1, piece).start()
        to_mate(down).start()
        if k <= LB:
            to_mate(up).start()
        for i, slot in enumerate(waiting):
            experts_in(slot, k == 1 and i == 0)
        waiting = [up, down] if k <= LB else [down]
        if k == 1:
            channel_norm()
        elif k == 2:
            c_both(steps.pop(0))
    c_both(steps.pop(0))
    if DN == 2:
        waiting = waiting + [turn((H - 1) * way)]
    for slot in waiting[:-1]:
        experts_in(slot, False)
    loads["ed"].wait()
    if len(steps) > 2:
        c_both(steps.pop(0))

    def m_mate(slot, piece):
        part = slice(None) if piece is None else pieces[piece]
        return remote(
            r.m_full.at[slot, part, other], r.m_pair.at[slot, part, :],
            r.out_sem.at[12], r.mm_in.at[slot if piece is None else Y + piece], mate,
        )

    def produce(slot):
        cols = pl.ds(pl.multiple_of(turn(y + slot) * 2 * F, 2 * F), 2 * F)
        r.m_full[slot] = dot(r.hidden[...], r.v_ed[:, cols]).astype(BF)
        m_mate(slot, None).start()

    def m_link(k, sign, piece):
        n, part = hop(k, sign), pieces[piece]
        return remote(
            r.m_stage.at[n, part, :], r.m_got.at[n, part, :],
            r.out_sem.at[13], r.m_in.at[n, piece], tp_of(sign * way),
        )

    def pair_sum(slot, piece):
        part = pieces[piece]
        return r.m_full[slot, part, mine].astype(F32) + r.m_pair[slot, part, :].astype(F32)

    def m_step(k, sign, piece):
        part = pieces[piece]
        total = pair_sum(turn(sign * k * way), piece)
        if k < (H if sign > 0 else H - 1):
            m_link(k + 1, sign, piece).wait_recv()
            total = total + r.m_got[hop(k + 1, sign), part, :].astype(F32)
        r.m_stage[hop(k, sign), part, :] = total.astype(BF)
        m_link(k, sign, piece).start()

    to_mate(waiting[-1]).wait_recv()
    far = H

    def wide(slot):
        return pl.ds(pl.multiple_of(turn(y + slot) * 2 * F, 2 * F), 2 * F)

    cols = wide(waiting[-1])
    wg, wu = r.v_eg[:, cols], r.v_eu[:, cols]
    for piece in (3, 2, 1, 0):
        part = pieces[piece]
        lhs = r.ag[waiting[-1], part, :]
        a = r.gate[part, :] + dot(lhs, wg, 1, 1)
        b = r.up[part, :] + dot(lhs, wu, 1, 1)
        hidden = (silu(a) * b).astype(BF)
        r.hidden[part, :] = hidden
        r.m_full[far, part, :] = dot(hidden, r.v_ed[:, wide(far)]).astype(BF)
        m_mate(far, piece).start()
    for slot in (turn(-(H - 1) * way), turn((H - 1) * way)):
        produce(slot)
    for piece in (3, 2, 1, 0):
        m_mate(far, piece).wait_recv()
        m_step(H, 1, piece)
    if H > 1:
        m_mate(turn(-(H - 1) * way), None).wait_recv()
        for piece in (3, 2, 1, 0):
            m_step(H - 1, -1, piece)
    if H > 2:
        for slot in (turn(-(H - 2) * way), turn((H - 2) * way)):
            produce(slot)
    for k in range(H - 1, 0, -1):
        m_mate(turn(k * way), None).wait_recv()
        for piece in (3, 2, 1, 0):
            m_step(k, 1, piece)
            if k > 1:
                if piece == 3:
                    m_mate(turn(-(k - 1) * way), None).wait_recv()
                m_step(k - 1, -1, piece)
        if k > 2:
            for slot in (turn(-(k - 2) * way), turn((k - 2) * way)):
                produce(slot)
        elif k == 2 or H == 2:
            produce(0)
        if k == g.C_AT and len(steps) > 1:
            c_both(steps.pop(0))

    m_mate(0, None).wait_recv()
    for piece in (3, 2, 1, 0):
        part = pieces[piece]
        total = pair_sum(0, piece)
        for sign in (1, -1):
            m_link(1, sign, piece).wait_recv()
            total = total + r.m_got[hop(1, sign), part, :].astype(F32)
        r.back[part, :] = total.astype(BF)
        if piece == 3:
            r.rows_ext[...] = total[M - cuts[3] :]
            for b in range(EX):
                r.back_ext[b] = r.rows_ext[b * EXT : (b + 1) * EXT, :].astype(BF)
            for b in range(EX - 1, 0, -1):
                remote(
                    r.back_ext.at[b], r.home_ext.at[opposite(b)],
                    r.out_sem.at[7], r.home_sem.at[1], peer(b),
                ).start()
        for b in range(EX * (piece + 1) // 4 - 1, max(EX * piece // 4, 1) - 1, -1):
            remote(
                r.back.at[pl.ds(b * MAIN, MAIN), :], r.home.at[pl.ds(opposite(b) * MAIN, MAIN), :],
                r.out_sem.at[6], r.home_sem.at[0], peer(b),
            ).start()
    r.home[0:MAIN, :] = r.back[0:MAIN, :]
    r.home_ext[0] = r.back_ext[0]

    while steps:
        c_both(steps.pop(0))
    total = c_sum(0)
    for sign in (1, -1):
        c_link(1, sign).wait_recv()
        total = total + r.c_got[hop(1, sign)].astype(F32)
    r.conv_out[...] = jnp.transpose(total).astype(BF)

    bulk(r.home_ext.at[pl.ds(1, EX - 1)], r.home_sem.at[1]).wait()
    for b in range(EX):
        r.rows_ext[b * EXT : (b + 1) * EXT, :] = r.home_ext[b].astype(F32)
    r.home[M:S, :] = r.rows_ext[...].astype(BF)
    bulk(r.home.at[pl.ds(MAIN, M - MAIN), :], r.home_sem.at[0]).wait()
    result = dot(r.w_hi[...], r.home[...], 0, 0) + dot(r.w_lo[...], r.home[...], 0, 0)
    r.moe_out[...] = result.astype(BF)

    bulk(r.send_main.at[0, pl.ds(MAIN, M - MAIN), :], r.out_sem.at[0]).wait()
    bulk(r.send_ext.at[0, pl.ds(1, EX - 1)], r.out_sem.at[1]).wait()
    if DN:
        bulk(r.send_main.at[pl.ds(1, DN), pl.ds(MAIN, M - MAIN), :], r.out_sem.at[2]).wait()
        bulk(r.send_ext.at[pl.ds(1, DN), pl.ds(1, EX - 1)], r.out_sem.at[3]).wait()
    halo.wait_send()
    bulk(r.stats.at[pl.ds(1, NT - 1)], r.out_sem.at[5]).wait()
    bulk(r.back.at[pl.ds(MAIN, M - MAIN), :], r.out_sem.at[6]).wait()
    bulk(r.back_ext.at[pl.ds(1, EX - 1)], r.out_sem.at[7]).wait()
    if LA + LB:
        bulk(r.ag.at[pl.ds(0, LA + LB), :, mine], r.out_sem.at[8]).wait()
    bulk(r.ag.at[:, :, mine], r.out_sem.at[9]).wait()
    bulk(r.c_part.at[pl.ds(0, Y)], r.out_sem.at[10]).wait()
    bulk(r.c_stage, r.out_sem.at[11]).wait()
    bulk(r.m_full.at[:, :, other], r.out_sem.at[12]).wait()
    bulk(r.m_stage, r.out_sem.at[13]).wait()


def run(Z, X, args):
    (tok_a, gain_a, vw, gw, ker, cg, ow, tok_b, gain_b, routes, logits, eg, eu, ed) = args
    EX, NT = lax.axis_size("ep"), lax.axis_size("tp")
    T, D = tok_a.shape
    R, F, HU = tok_b.shape[0], vw.shape[1], eg.shape[2]
    cap = 3 * R * routes.shape[1] // (2 * EX)
    EXT, Y, DN = cap - MAIN, NT // 2, 2
    S, M = EX * cap, EX * MAIN
    given = dict(
        tok_b=tok_b, routes=routes.T, logits=logits.T, gain_b=gain_b.reshape(NT, F),
        tok_a=tok_a, gain_a=gain_a.reshape(NT, F), vw=vw, gw=gw, ker=ker, cg=cg.reshape(1, F),
        ow=ow, eg=eg[0].T, eu=eu[0].T, ed=ed[0],
    )
    vm, dma = pltpu.VMEM, pltpu.SemaphoreType.DMA
    scratch = dict(
        {"v_" + n: vm(given[n].shape, given[n].dtype) for n in INPUTS},
        in_sem=dma((len(INPUTS),)), spread=vm((EX + 8, S), BF), code=vm((EX + 8, R), F32),
        picks=vm((S, R), BF), weight=vm((EX, R), F32), w_hi=vm((S, R), BF), w_lo=vm((S, R), BF),
        send_main=vm((DN + 1, M, F), BF), send_ext=vm((DN + 1, EX, EXT, F), BF),
        recv_ext=vm((DN + 1, EX, EXT, F), BF),
        rows_ext=vm((EX * EXT, F), F32), ag=vm((Y, S, 2 * F), BF),
        out_sem=dma((14,)), a2a_sem=dma((5,)), normed_a=vm((T, D), BF), padded=vm((T + 32, F), F32),
        tail=vm((32, F), BF), halo=vm((32, F), BF), halo_sem=dma, mixed=vm((T, F), F32),
        stats=vm((NT, 2, T), F32), stat_sem=dma,
        ag_in=dma((max(Y - 1 - DN, 1), 4)), am_in=dma((Y,)),
        c_part=vm((NT, T, F), BF), c_pair=vm((Y, T, F), BF), c_stage=vm((Y - 1, T, F), BF),
        c_got=vm((Y - 1, T, F), BF), cm_in=dma, c_in=dma((Y - 1,)),
        gate=vm((S, HU), F32), up=vm((S, HU), F32), hidden=vm((S, HU), BF),
        m_full=vm((Y, S, 2 * F), BF), m_pair=vm((Y, S, F), BF), m_stage=vm((Y - 1, S, F), BF),
        m_got=vm((Y - 1, S, F), BF), mm_in=dma((Y + 4,)), m_in=dma((Y - 1, 4)), back=vm((S, F), BF), back_ext=vm((EX, EXT, F), BF),
        home=vm((S, F), BF), home_ext=vm((EX, EXT, F), BF), home_sem=dma((2,)),
    )
    names = ["in_" + n for n in INPUTS] + ["conv_out", "moe_out"] + list(scratch)
    g = SimpleNamespace(
        names=names, Z=Z, X=X, Y=Y, F=F, EX=EX, EXT=EXT, NT=NT, T=T, R=R, D=D, S=S, CH=NT * F,
        TAPS=ker.shape[0], TILES=3, DN=DN, DIRECT_AT=max(NT // 4 - (DN + 1) // 2, 1), C_AT=2,
    )
    conv_out, moe_out = pl.pallas_call(
        functools.partial(kernel, g),
        out_shape=(pltpu.VMEM((F, T), BF), pltpu.VMEM((R, F), BF)),
        in_specs=[pl.BlockSpec(memory_space=pl.ANY)] * len(INPUTS),
        out_specs=(pl.BlockSpec(memory_space=pltpu.VMEM),) * 2,
        scratch_shapes=list(scratch.values()),
        compiler_params=pltpu.CompilerParams(
            collective_id=0, has_side_effects=True, vmem_limit_bytes=60 * 1024 * 1024
        ),
    )(*[given[n] for n in INPUTS])
    return conv_out, moe_out.T


def solution(mesh, Z=8, X=4):
    return jax.shard_map(
        lambda *args: run(Z, X, args),
        mesh=mesh,
        in_specs=(
            P("ep", None), P(), P(None, "tp"), P(None, "tp"), P(None, "tp"), P("tp"), P("tp", None),
            P("ep", None), P(), P("ep", None), P("ep", None), P("ep", None, "tp"),
            P("ep", None, "tp"), P("ep", "tp", None),
        ),
        out_specs=(P("tp", "ep"), P("tp", "ep")),
        check_vma=False,
    )
```

time: 66 us -> 62.8 us (0.952)
  Pallas kernels: 64 us -> 60.8 us
    pallas_call x1, Pallas kernels: 64 us -> 60.8 us  [run(): pl.pallas_call(functools.partial(kernel, g), out_shape=(pltpu.VMEM((F, T)...]
where the time goes in v4:
time: 62.8 us; the launch traced here: 62.7 us
  Pallas kernels  60.8 us (97%)
  local copies, waits for them, and re-layouts  1.24 us (2%)
  between operations  0.64 us (1%)
    pallas_call x1, Pallas kernels, run(): pl.pallas_call(functools.partial(kernel, g), out_shape=(pltpu.VMEM((F, T)...  60.8 us

profile of v4, /device:TPU:1, one launch (start us, length us, event | category | flops | bytes accessed | tf_op | source)
XLA Modules:
  0.0 62.7 jit_solution(3717887843504359620)
XLA Ops:
  0.6 60.8 %shard_map.149 = (bf16[128,128]{1,0:T(8,128)(2,1)S(1)}, bf16[192,128]{1,0:T(8,128)(2,1)S(1)}) custom-call(s32[2,192]{1,0:T(2,128)} %bitcast.19, f32[2,192]{1,0:T(2,128)} %bitcast.20, bf16[192,2048]{1,0:T(8,128)(2,1)} %refs_2_.1, f32[16,128]{1,0:T(8,128)} %bitcast.17, bf16[128,2048]{1,0:T(8,128)(2,1)} %refs_4_.1, f32[16,128]{1,0:T(8,128)} %bitcast.18, ...), custom_call_target="tpu_custom_call" | custom-call | tf_op jit(solution)/shard_map/pallas_call | solution.py:539
  61.5 0.6 copy.18
  62.1 0.6 copy.19

commit v5 on v4

--- a/solution.py
+++ b/solution.py
@@ -173,6 +173,60 @@
     halo = remote(r.tail, r.halo, r.out_sem.at[4], r.halo_sem, (lax.rem(e + 1, EX), t))
     halo.start()
 
+    weight = r.weight[...]
+    w_hi = weight.astype(BF)
+    w_lo = (weight - w_hi.astype(F32)).astype(BF)
+    r.w_hi[...] = (r.picks[...].astype(F32) * dot(r.spread[0:EX, :], w_hi, 0, 0)).astype(BF)
+    r.w_lo[...] = (r.picks[...].astype(F32) * dot(r.spread[0:EX, :], w_lo, 0, 0)).astype(BF)
+
+    cuts = [(EX * i // 4) * MAIN for i in range(4)] + [S]
+    pieces = [pl.ds(a, b - a) for a, b in zip(cuts, cuts[1:])]
+
+    def pass_on(sign, k, piece):
+        return remote(
+            r.ag.at[turn(-sign * (k - 1) * way), pieces[piece], mine],
+            r.ag.at[turn(-sign * k * way), pieces[piece], mine],
+            r.out_sem.at[8], r.ag_in.at[k - 1 if sign > 0 else LA + k - 1, piece], tp_of(sign * way),
+        )
+
+    def to_mate(slot):
+        return remote(
+            r.ag.at[slot, :, mine], r.ag.at[slot, :, mine], r.out_sem.at[9], r.am_in.at[slot], mate
+        )
+
+    def bulk(ref, sem):
+        return pltpu.make_async_copy(ref, ref, sem)
+
+    def settle_ext(i, slot):
+        for b in range(EX):
+            r.rows_ext[b * EXT : (b + 1) * EXT, :] = r.recv_ext[i, b].astype(F32)
+        r.ag[slot, M:S, mine] = r.rows_ext[...].astype(BF)
+
+    def convolve():
+        loads["ker"].wait()
+        halo.wait_recv()
+        r.padded[0:32, :] = jnp.where(e > 0, r.halo[...].astype(F32), 0.0)
+        mixed = jnp.zeros((T, F), F32)
+        for tap in range(g.TAPS):
+            low = 32 - (g.TAPS - 1) + tap
+            mixed = mixed + r.v_ker[tap : tap + 1, :] * r.padded[low : low + T, :]
+        r.mixed[...] = mixed
+        ones = jnp.ones((8, F), F32)
+        sums = dot(ones, mixed, 1, 1, lax.Precision.HIGHEST)
+        powers = dot(ones, mixed * mixed, 1, 1, lax.Precision.HIGHEST)
+        r.stats[0] = jnp.where(iota((8, T), 0) == 0, sums, powers)[0:2]
+
+        for i in range(1, NT):
+            remote(
+                r.stats.at[0], r.stats.at[NT - i], r.out_sem.at[5], r.stat_sem, tps[i]
+            ).start()
+
+    bulk(r.ag.at[0, pl.ds(MAIN, HALF - MAIN), mine], r.a2a_sem.at[0]).wait()
+    for piece in (0, 1):
+        if LA:
+            pass_on(1, 1, piece).start()
+        if LB:
+            pass_on(-1, 1, piece).start()
     for i in range(DN):
         rows_for(1 + i, near + i)
     for b in range(1, EX if DN else 0):
@@ -186,60 +240,6 @@
             r.send_ext.at[pl.ds(1, DN), b], r.recv_ext.at[pl.ds(1, DN), nb],
             r.out_sem.at[3], r.a2a_sem.at[4], peer(b),
         ).start()
-    weight = r.weight[...]
-    w_hi = weight.astype(BF)
-    w_lo = (weight - w_hi.astype(F32)).astype(BF)
-    r.w_hi[...] = (r.picks[...].astype(F32) * dot(r.spread[0:EX, :], w_hi, 0, 0)).astype(BF)
-    r.w_lo[...] = (r.picks[...].astype(F32) * dot(r.spread[0:EX, :], w_lo, 0, 0)).astype(BF)
-
-    cuts = [(EX * i // 4) * MAIN for i in range(4)] + [S]
-    pieces = [pl.ds(a, b - a) for a, b in zip(cuts, cuts[1:])]
-
-    def pass_on(sign, k, piece):
-        return remote(
-            r.ag.at[turn(-sign * (k - 1) * way), pieces[piece], mine],
-            r.ag.at[turn(-sign * k * way), pieces[piece], mine],
-            r.out_sem.at[8], r.ag_in.at[k - 1 if sign > 0 else LA + k - 1, piece], tp_of(sign * way),
-        )
-
-    def to_mate(slot):
-        return remote(
-            r.ag.at[slot, :, mine], r.ag.at[slot, :, mine], r.out_sem.at[9], r.am_in.at[slot], mate
-        )
-
-    def bulk(ref, sem):
-        return pltpu.make_async_copy(ref, ref, sem)
-
-    def settle_ext(i, slot):
-        for b in range(EX):
-            r.rows_ext[b * EXT : (b + 1) * EXT, :] = r.recv_ext[i, b].astype(F32)
-        r.ag[slot, M:S, mine] = r.rows_ext[...].astype(BF)
-
-    def convolve():
-        loads["ker"].wait()
-        halo.wait_recv()
-        r.padded[0:32, :] = jnp.where(e > 0, r.halo[...].astype(F32), 0.0)
-        mixed = jnp.zeros((T, F), F32)
-        for tap in range(g.TAPS):
-            low = 32 - (g.TAPS - 1) + tap
-            mixed = mixed + r.v_ker[tap : tap + 1, :] * r.padded[low : low + T, :]
-        r.mixed[...] = mixed
-        ones = jnp.ones((8, F), F32)
-        sums = dot(ones, mixed, 1, 1, lax.Precision.HIGHEST)
-        powers = dot(ones, mixed * mixed, 1, 1, lax.Precision.HIGHEST)
-        r.stats[0] = jnp.where(iota((8, T), 0) == 0, sums, powers)[0:2]
-
-        for i in range(1, NT):
-            remote(
-                r.stats.at[0], r.stats.at[NT - i], r.out_sem.at[5], r.stat_sem, tps[i]
-            ).start()
-
-    bulk(r.ag.at[0, pl.ds(MAIN, HALF - MAIN), mine], r.a2a_sem.at[0]).wait()
-    for piece in (0, 1):
-        if LA:
-            pass_on(1, 1, piece).start()
-        if LB:
-            pass_on(-1, 1, piece).start()
     convolve()
     bulk(r.ag.at[0, pl.ds(HALF, HALF), mine], r.a2a_sem.at[1]).wait()
     bulk(r.recv_ext.at[0, pl.ds(1, EX - 1)], r.a2a_sem.at[2]).wait()
@@ -412,11 +412,12 @@
         r.hidden[part, :] = hidden
         r.m_full[far, part, :] = dot(hidden, r.v_ed[:, wide(far)]).astype(BF)
         m_mate(far, piece).start()
-    for slot in (turn(-(H - 1) * way), turn((H - 1) * way)):
-        produce(slot)
     for piece in (3, 2, 1, 0):
         m_mate(far, piece).wait_recv()
         m_step(H, 1, piece)
+        if piece == 3:
+            produce(turn(-(H - 1) * way))
+    produce(turn((H - 1) * way))
     if H > 1:
         m_mate(turn(-(H - 1) * way), None).wait_recv()
         for piece in (3, 2, 1, 0):
@@ -452,16 +453,17 @@
             r.rows_ext[...] = total[M - cuts[3] :]
             for b in range(EX):
                 r.back_ext[b] = r.rows_ext[b * EXT : (b + 1) * EXT, :].astype(BF)
+        for b in range(EX * (piece + 1) // 4 - 1, max(EX * piece // 4, 1) - 1, -1):
+            remote(
+                r.back.at[pl.ds(b * MAIN, MAIN), :], r.home.at[pl.ds(opposite(b) * MAIN, MAIN), :],
+                r.out_sem.at[6], r.home_sem.at[0], peer(b),
+            ).start()
+        if piece == 3:
             for b in range(EX - 1, 0, -1):
                 remote(
                     r.back_ext.at[b], r.home_ext.at[opposite(b)],
                     r.out_sem.at[7], r.home_sem.at[1], peer(b),
                 ).start()
-        for b in range(EX * (piece + 1) // 4 - 1, max(EX * piece // 4, 1) - 1, -1):
-            remote(
-                r.back.at[pl.ds(b * MAIN, MAIN), :], r.home.at[pl.ds(opposite(b) * MAIN, MAIN), :],
-                r.out_sem.at[6], r.home_sem.at[0], peer(b),
-            ).start()
     r.home[0:MAIN, :] = r.back[0:MAIN, :]
     r.home_ext[0] = r.back_ext[0]
 

time: 62.8 us -> 62.1 us (0.989); the launches traced: 62.7 us -> 61.3 us
  Pallas kernels: 60.8 us -> 59.4 us
    pallas_call x1, Pallas kernels: 60.8 us -> 59.4 us  [run(): pl.pallas_call(functools.partial(kernel, g), out_shape=(pltpu.VMEM((F, T)...]
where the time goes in v5:
time: 62.1 us; the launch traced here: 61.3 us
  Pallas kernels  59.4 us (96%)
  local copies, waits for them, and re-layouts  1.24 us (2%)
  between operations  0.64 us (1%)
    pallas_call x1, Pallas kernels, run(): pl.pallas_call(functools.partial(kernel, g), out_shape=(pltpu.VMEM((F, T)...  59.4 us

profile of v5, /device:TPU:1, one launch (start us, length us, event | category | flops | bytes accessed | tf_op | source)
XLA Modules:
  0.0 61.3 jit_solution(1675576068148042806)
XLA Ops:
  0.6 59.4 %shard_map.149 = (bf16[128,128]{1,0:T(8,128)(2,1)S(1)}, bf16[192,128]{1,0:T(8,128)(2,1)S(1)}) custom-call(s32[2,192]{1,0:T(2,128)} %bitcast.19, f32[2,192]{1,0:T(2,128)} %bitcast.20, bf16[192,2048]{1,0:T(8,128)(2,1)} %refs_2_.1, f32[16,128]{1,0:T(8,128)} %bitcast.17, bf16[128,2048]{1,0:T(8,128)(2,1)} %refs_4_.1, f32[16,128]{1,0:T(8,128)} %bitcast.18, ...), custom_call_target="tpu_custom_call" | custom-call | tf_op jit(solution)/shard_map/pallas_call | solution.py:541
  60.0 0.6 %copy.18 = bf16[128,128]{1,0:T(8,128)(2,1)} copy(bf16[128,128]{1,0:T(8,128)(2,1)S(1)} %get-tuple-element.6) | data formatting | bytes 65536
  60.7 0.6 %copy.19 = bf16[128,192]{0,1:T(8,128)(2,1)} copy(bf16[128,192]{0,1:T(8,128)(2,1)S(1)} %bitcast.13) | data formatting | bytes 98304

commit v6 on v5

--- a/solution.py
+++ b/solution.py
@@ -334,9 +334,15 @@
 
     for k in range(1, LA + 1):
         if DN and k == g.DIRECT_AT:
-            waiting = waiting + take_direct()
+            if k > 1:
+                early, waiting = waiting, take_direct()
+            else:
+                waiting = waiting + take_direct()
         down, up = turn(-k * way), turn(k * way)
         for piece in range(4):
+            if k == LA and k > 1 and piece == 2:
+                for slot in early:
+                    experts_in(slot, False)
             pass_on(1, k, piece).wait_recv()
             if k < LA:
                 pass_on(1, k + 1, piece).start()
@@ -536,7 +542,7 @@
     names = ["in_" + n for n in INPUTS] + ["conv_out", "moe_out"] + list(scratch)
     g = SimpleNamespace(
         names=names, Z=Z, X=X, Y=Y, F=F, EX=EX, EXT=EXT, NT=NT, T=T, R=R, D=D, S=S, CH=NT * F,
-        TAPS=ker.shape[0], TILES=3, DN=DN, DIRECT_AT=max(NT // 4 - (DN + 1) // 2, 1), C_AT=2,
+        TAPS=ker.shape[0], TILES=3, DN=DN, DIRECT_AT=max(NT // 4 - (DN + 1) // 2, 1), C_AT=1,
     )
     conv_out, moe_out = pl.pallas_call(
         functools.partial(kernel, g),

time: 62.1 us -> 61.8 us (level)
  no operation moved by 1% of the time
where the time goes in v6:
time: 61.8 us; the launch traced here: 60.7 us
  Pallas kernels  58.9 us (95%)
  local copies, waits for them, and re-layouts  1.24 us (2%)
  between operations  0.64 us (1%)
    pallas_call x1, Pallas kernels, run(): pl.pallas_call(functools.partial(kernel, g), out_shape=(pltpu.VMEM((F, T)...  58.9 us
    unnamed x2, local copies, waits for them, and re-layouts  1.24 us

profile of v6, /device:TPU:1, one launch (start us, length us, event | category | flops | bytes accessed | tf_op | source)
XLA Modules:
  0.0 60.7 jit_solution(13396134060617934084)
XLA Ops:
  0.6 58.9 %shard_map.149 = (bf16[128,128]{1,0:T(8,128)(2,1)S(1)}, bf16[192,128]{1,0:T(8,128)(2,1)S(1)}) custom-call(s32[2,192]{1,0:T(2,128)} %bitcast.19, f32[2,192]{1,0:T(2,128)} %bitcast.20, bf16[192,2048]{1,0:T(8,128)(2,1)} %refs_2_.1, f32[16,128]{1,0:T(8,128)} %bitcast.17, bf16[128,2048]{1,0:T(8,128)(2,1)} %refs_4_.1, f32[16,128]{1,0:T(8,128)} %bitcast.18, ...), custom_call_target="tpu_custom_call" | custom-call | tf_op jit(solution)/shard_map/pallas_call | solution.py:547
  59.5 0.6 %copy.18 = bf16[128,128]{1,0:T(8,128)(2,1)} copy(bf16[128,128]{1,0:T(8,128)(2,1)S(1)} %get-tuple-element.6) | data formatting | bytes 65536
  60.1 0.6 %copy.19 = bf16[128,192]{0,1:T(8,128)(2,1)} copy(bf16[128,192]{0,1:T(8,128)(2,1)S(1)} %bitcast.13) | data formatting | bytes 98304
